TPU v7x, 256 devices: a 4x2x16 block of a 4x16x16 slice. The times are simulated.
256 devices in a mesh: grp: 2 (over y), sp: 32 (over z, core), tp: 4 (over x).
Axes of the slice: x: 4, y: 2, z: 16, core: 2. Of those that a mesh axis runs over, the one named last changes fastest.
The devices are a block of a 4x16x16 slice.
Arguments:
- query_nope: bfloat16 [20480, 1024], P(('grp', 'sp'), 'tp'), parts along dimension 0, may hold values from -12 to 12
- query_rope: bfloat16 [20480, 512], P(('grp', 'sp'), 'tp'), parts along dimension 0, may hold values from -48 to 48
- token_latent: bfloat16 [20480, 256], P(('grp', 'sp')), parts along dimension 0, may hold values from -6 to 6
- key_rope: bfloat16 [20480, 32], P(('grp', 'sp')), parts along dimension 0, may hold values from -48 to 48
- latent_norm_gain: float32 [256], replicated, may hold values from 0.1 to 1.9
- key_expand_weight: bfloat16 [256, 1024], replicated, may hold values from -0.375 to 0.375
- value_expand_weight: bfloat16 [256, 1024], replicated, may hold values from -0.375 to 0.375
- residual: bfloat16 [20480, 2048], P(('grp', 'sp')), parts along dimension 0, may hold values from -3 to 3
- out_weight: bfloat16 [1024, 2048], P('tp'), may hold values from -0.375 to 0.375
- ffn_gain: float32 [2048], replicated, may hold values from 0.1 to 1.9
- gate_weight: bfloat16 [2048, 5632], P('sp', 'tp'), may hold values from -0.125 to 0.125
- up_weight: bfloat16 [2048, 5632], P('sp', 'tp'), may hold values from -0.125 to 0.125
- down_weight: bfloat16 [5632, 2048], P('tp', 'sp'), may hold values from -0.078125 to 0.078125
Outputs:
- layer_output: bfloat16 [20480, 2048], P(('grp', 'sp', 'tp')), parts along dimension 0
There are 2 independent parts, one for each index of `grp`. A program takes and returns all parts, laid end to end along the dimension named above; an argument that names none is the same for every part. Nothing has to cross between parts.
All inputs are finite; a program needn't handle non-finite values.
Results may differ from a plain program's by a relative error of at most 0.015.
Values may be sent and summed in bfloat16 or wider, within the bound.
No kernel may reach another device: no remote copies, remote signals or barrier semaphores. Data moves between devices by JAX's collectives and lax.ppermute only.
A program may use at most 128 MiB of HBM per device.

v0:
```python
import jax
import jax.numpy as jnp
from jax import lax
from jax.sharding import PartitionSpec as P

UNROTATED_SIZE = 64
ROPE = 32
VALUE_SIZE = 64
GRID_W = 64


def side_by_side(arrays, axis, dim, along):
    widths = [a.shape[along] for a in arrays]
    both = jnp.concatenate(arrays, axis=along)
    whole = lax.all_gather(both, axis, axis=dim, tiled=True)
    return tuple(jnp.split(whole, [sum(widths[:k]) for k in range(1, len(widths))], axis=along))


def cut_along(array, dim, count):
    dims = array.shape
    parts = array.reshape(*dims[:dim], count, dims[dim] // count, *dims[dim + 1 :])
    return jnp.moveaxis(parts, dim, 0)


def summed_on_arrival(array, axis, dim):
    count = lax.axis_size(axis)
    parts = lax.all_to_all(cut_along(array, dim, count), axis, 0, 0, tiled=True)
    return jnp.sum(parts.astype(jnp.float32), axis=0)


def sent_to_all(array, axis):
    copies = jnp.broadcast_to(array, (lax.axis_size(axis), *array.shape))
    return lax.all_to_all(copies, axis, split_axis=0, concat_axis=0, tiled=True)


def joined_along(parts, dim):
    dims = list(parts.shape[1:])
    dims[dim] *= parts.shape[0]
    return jnp.moveaxis(parts, 0, dim).reshape(dims)


def collect(array, axis, dim):
    parts = sent_to_all(array, axis)
    return joined_along(parts, dim)


def norm_rows(values, gain):
    wide = values.astype(jnp.float32)
    return wide * lax.rsqrt(jnp.mean(wide * wide, axis=-1, keepdims=True) + 1e-06) * gain


def turn_heads(vectors, positions):
    tokens, heads, width = vectors.shape
    freqs = width // 4
    grid_pos = jnp.stack([positions // GRID_W, positions % GRID_W], axis=-1).astype(jnp.float32)
    inverse = jnp.power(10000.0, -jnp.arange(freqs, dtype=jnp.float32) / freqs)
    angles = grid_pos[:, :, None] * inverse
    cosine = jnp.cos(angles)[:, None]
    sine = jnp.sin(angles)[:, None]
    viewed = vectors.reshape(tokens, heads, 2, 2, freqs)
    first = viewed[..., 0, :]
    second = viewed[..., 1, :]
    turned = jnp.stack([first * cosine - second * sine, first * sine + second * cosine], axis=-2)
    return turned.reshape(tokens, heads, width)


def local(
    query_nope,
    query_rope,
    token_latent,
    key_rope,
    latent_norm_gain,
    key_expand_weight,
    value_expand_weight,
    residual,
    out_weight,
    ffn_gain,
    gate_weight,
    up_weight,
    down_weight,
):
    tok_rows = query_nope.shape[0]
    heads_here = query_nope.shape[1] // UNROTATED_SIZE
    own_rows = tok_rows // lax.axis_size("tp")
    tp_index = lax.axis_index("tp")
    positions = lax.axis_index("sp") * tok_rows + jnp.arange(tok_rows, dtype=jnp.int32)
    gate_full, up_full = side_by_side((gate_weight, up_weight), "sp", 0, 1)
    query_flat = query_nope.reshape(tok_rows, heads_here, UNROTATED_SIZE)
    query_turned = turn_heads(
        query_rope.astype(jnp.float32).reshape(tok_rows, heads_here, ROPE), positions
    ).astype(jnp.bfloat16)
    latent = norm_rows(token_latent, latent_norm_gain).astype(jnp.bfloat16)
    key_turned = turn_heads(key_rope.astype(jnp.float32)[:, None, :], positions)[:, 0].astype(
        jnp.bfloat16
    )
    key_cols = lax.dynamic_slice_in_dim(
        key_expand_weight, tp_index * heads_here * UNROTATED_SIZE, heads_here * UNROTATED_SIZE, 1
    )
    value_cols = lax.dynamic_slice_in_dim(
        value_expand_weight, tp_index * heads_here * VALUE_SIZE, heads_here * VALUE_SIZE, 1
    )
    score_scale = (UNROTATED_SIZE + ROPE) ** (-0.5)

    def absorb(carried, block_in):
        latent_block, rope_block = block_in
        block_rows = latent_block.shape[0]
        key_rows = jnp.dot(latent_block, key_cols, preferred_element_type=jnp.float32).astype(
            jnp.bfloat16
        )
        key_rows = key_rows.reshape(block_rows, heads_here, UNROTATED_SIZE)
        value_rows = jnp.dot(latent_block, value_cols, preferred_element_type=jnp.float32).astype(
            jnp.bfloat16
        )
        value_rows = value_rows.reshape(block_rows, heads_here, VALUE_SIZE)
        scores = (
            jnp.einsum("qhd,khd->hqk", query_flat, key_rows, preferred_element_type=jnp.float32)
            + jnp.einsum(
                "qhd,kd->hqk", query_turned, rope_block, preferred_element_type=jnp.float32
            )
        ) * score_scale
        highest, totals, accumulated = carried
        new_highest = jnp.maximum(highest, jnp.max(scores, axis=-1))
        shrink = jnp.exp(highest - new_highest)
        weights = jnp.exp(scores - new_highest[:, :, None])
        totals = totals * shrink + jnp.sum(weights, axis=-1)
        accumulated = accumulated * shrink.T[:, :, None] + jnp.einsum(
            "hqk,khd->qhd",
            weights.astype(jnp.bfloat16),
            value_rows,
            preferred_element_type=jnp.float32,
        )
        return ((new_highest, totals, accumulated), None)

    initial = (
        jnp.full((heads_here, tok_rows), -jnp.inf, jnp.float32),
        jnp.zeros((heads_here, tok_rows), jnp.float32),
        jnp.zeros((tok_rows, heads_here, VALUE_SIZE), jnp.float32),
    )
    carried = initial
    latent_piece = lax.all_gather(latent, "sp", axis=0, tiled=True)
    rope_piece = lax.all_gather(key_turned, "sp", axis=0, tiled=True)
    shard_count = latent_piece.shape[0] // tok_rows
    grouped = max(
        (
            factor
            for factor in range(1, shard_count + 1)
            if shard_count % factor == 0 and factor * tok_rows <= max(1024, tok_rows)
        )
    )
    block_rows = grouped * tok_rows
    blocks = (
        latent_piece.reshape(-1, block_rows, latent_piece.shape[1]),
        rope_piece.reshape(-1, block_rows, rope_piece.shape[1]),
    )
    carried, _ = lax.scan(absorb, carried, blocks)
    highest, totals, accumulated = carried
    attended = (
        (accumulated / totals.T[:, :, None])
        .reshape(tok_rows, heads_here * VALUE_SIZE)
        .astype(jnp.bfloat16)
    )
    head_sum = summed_on_arrival(
        jnp.dot(attended, out_weight, preferred_element_type=jnp.float32).astype(jnp.bfloat16),
        "tp",
        0,
    )
    mixed_own = (
        lax.dynamic_slice_in_dim(residual, tp_index * own_rows, own_rows, 0).astype(jnp.float32)
        + head_sum
    )
    normed_own = norm_rows(mixed_own, ffn_gain).astype(jnp.bfloat16)
    normed_all = collect(normed_own, "tp", 0)
    gate = jnp.dot(normed_all, gate_full, preferred_element_type=jnp.float32)
    up_part = jnp.dot(normed_all, up_full, preferred_element_type=jnp.float32)
    hidden = (jax.nn.silu(gate) * up_part).astype(jnp.bfloat16)
    terms = jnp.dot(
        hidden,
        lax.all_gather(down_weight, "sp", axis=1, tiled=True),
        preferred_element_type=jnp.float32,
    )
    ffn_own = summed_on_arrival(terms.astype(jnp.bfloat16), "tp", 0)
    return (mixed_own + ffn_own).astype(jnp.bfloat16)


def solution(mesh):
    return jax.shard_map(
        local,
        mesh=mesh,
        in_specs=(
            P(("grp", "sp"), "tp"),
            P(("grp", "sp"), "tp"),
            P(("grp", "sp"), None),
            P(("grp", "sp"), None),
            P(),
            P(),
            P(),
            P(("grp", "sp"), None),
            P("tp", None),
            P(),
            P("sp", "tp"),
            P("sp", "tp"),
            P("tp", "sp"),
        ),
        out_specs=P(("grp", "sp", "tp"), None),
        check_vma=False,
    )
```

profile of v0, /device:TPU:40, one launch (start us, length us, event | category | flops | bytes accessed | tf_op | source)
XLA Modules:
  0.0 341.1 jit_solution(13385910839321723179)
XLA Ops:
  15.8 52.6 %all-gather = bf16[32,320,32]{1,2,0:T(8,128)(2,1)S(1)} all-gather(bf16[1,320,32]{1,2,0:T(8,128)(2,1)S(1)} %bitcast.89), channel_id=1, replica_groups=mesh['grp'=2,'sp'=32,'tp'=4] {'sp'}, dimensions={0}, use_global_device_ids=true | all-gather | bytes 675840 | tf_op jit(solution)/shard_map/all_gather | solution.py:141
  72.4 24.7 %all-gather.5.cloned.1.call-done = bf16[10240,256]{1,0:T(8,128)(2,1)} async-done(((bf16[320,256]{1,0:T(8,128)(2,1)}), bf16[10240,256]{1,0:T(8,128)(2,1)}) %all-gather.5.cloned.1.call-update) | async-done | bytes 5242896 | tf_op jit(solution)/shard_map/all_gather | solution.py:140
  97.1 152.5 %while.15 = (s32[]{:T(128)}, f32[4,320]{1,0:T(4,128)S(1)}, f32[4,320]{1,0:T(4,128)S(1)}, f32[320,4,64]{0,2,1:T(8,128)S(1)}, bf16[16,640,256]{2,1,0:T(8,128)(2,1)...) while((s32[]{:T(128)}, f32[4,320]{1,0:T(4,128)S(1)}, ...), condition=%wide.region_4.5_spmd.clone, body=%wide.region_1.4_spmd.clone.sunk | while | flops 436231680 | bytes 32760992 | solution.py:155
  102.9 2.7 fusion.90
  108.5 2.4 fusion.86
  112.4 2.7 fusion.90
  118.0 2.4 fusion.86
  121.9 2.8 fusion.90
  127.5 2.4 fusion.86
  131.4 2.7 fusion.90
  140.9 2.8 fusion.90
  146.6 2.4 fusion.86
  150.5 2.8 fusion.90
  160.1 2.8 fusion.90
  165.7 2.4 fusion.86
  169.6 2.8 fusion.90
  179.2 2.7 fusion.90
  188.7 2.9 fusion.90
  198.3 2.8 fusion.90
  203.9 2.4 fusion.86
  207.8 2.7 fusion.90
  217.3 2.8 fusion.90
  226.8 2.8 fusion.90
  232.5 2.4 fusion.86
  236.4 2.7 fusion.90
  245.9 2.8 fusion.90
  251.2 4.2 %all-to-all-start = ((bf16[4,80,2048]{2,1,0:T(8,128)(2,1)}), bf16[4,80,2048]{2,1,0:T(8,128)(2,1)S(1)}, u32[]{:S(2)}, u32[]{:S(2)}) async-start(bf16[4,80,2048]{2,1,0:T(8,128)(2,1)} %bitcast.80), calls=%async_computation | async-start | bytes 2621440 | tf_op jit(solution)/shard_map/all_to_all | solution.py:27
  255.4 18.3 %all-to-all-done = bf16[4,80,2048]{2,1,0:T(8,128)(2,1)S(1)} async-done(((bf16[4,80,2048]{2,1,0:T(8,128)(2,1)}), bf16[4,80,2048]{2,1,0:T(8,128)(2,1)S(1)}, u32[]{:S(2)}, u32[]{:S(2)}) %all-to-all-start) | async-done | bytes 1310752 | tf_op jit(solution)/shard_map/all_to_all | solution.py:27
  276.4 20.0 %all_to_all.15 = bf16[4,80,2048]{2,1,0:T(8,128)(2,1)S(1)} all-to-all(bf16[4,80,2048]{2,1,0:T(8,128)(2,1)S(1)} %broadcast_in_dim.11), channel_id=1, replica_groups=mesh['grp'=2,'sp'=32,'tp'=4] {'tp'}, dimensions={0} | all-to-all | bytes 2621440 | tf_op jit(solution)/shard_map/all_to_all | solution.py:33
  296.4 6.1 %fusion.25 = f32[320,1408]{1,0:T(8,128)} fusion(bf16[320,2048]{1,0:T(8,128)(2,1)S(1)} %bitcast.83, bf16[2048,2816]{1,0:T(8,128)(2,1)} %all-gather.7.cloned.1.call-done), kind=kOutput, calls=%fused_computation.28 | convolution fusion | flops 1845493760 | bytes 8880128 | tf_op jit(solution)/shard_map/dot_general | solution.py:173
  302.5 10.2 %convolution_convert_fusion.2 = bf16[320,2048]{1,0:T(8,128)(2,1)} fusion(bf16[1408,2048]{0,1:T(8,128)(2,1)} %all-gather.9.cloned.1.call-done, bf16[320,2048]{1,0:T(8,128)(2,1)S(1)} %bitcast.84, bf16[2048,2816]{1,0:T(8,128)(2,1)} %all-gather.7.cloned.1.call-done, f32[320,1408]{1,0:T(8,128)} %fusion.25), kind=kOutput, calls=%fused_computation.31 | convolution fusion | flops 3694346240 | bytes 15958016 | tf_op jit(solution)/shard_map/dot_general | solution.py:176
  312.6 19.9 %all_to_all.16 = bf16[4,80,2048]{2,1,0:T(8,128)(2,1)S(1)} all-to-all(bf16[4,80,2048]{2,1,0:T(8,128)(2,1)} %bitcast.85), channel_id=1, replica_groups=mesh['grp'=2,'sp'=32,'tp'=4] {'tp'}, dimensions={0} | all-to-all | bytes 2621440 | tf_op jit(solution)/shard_map/all_to_all | solution.py:27
  (197 shorter events, 109.4 us)
Async XLA Ops:
  6.5 243.1 %copy-start = (bf16[256,2048]{1,0:T(8,128)(2,1)S(1)}, bf16[256,2048]{1,0:T(8,128)(2,1)}, u32[]{:S(2)}) copy-start(bf16[256,2048]{1,0:T(8,128)(2,1)} %param.23) | copy-start | bytes 3145732
  6.6 90.5 %all-gather.5.cloned.1.call-start = ((), (), s32[]{:S(2)}) async-start(), calls=%async_computation.3 | async-start | bytes 5406720 | tf_op jit(solution)/shard_map/all_gather | solution.py:140
  9.5 286.9 %all-gather.7.cloned.1.call-start = ((), (), s32[]{:S(2)}) async-start(), calls=%async_computation.4 | async-start | bytes 11894784 | tf_op jit(solution)/shard_map/all_gather | solution.py:15
  11.4 291.0 %all-gather.9.cloned.1.call-start = ((), (), s32[]{:S(2)}) async-start(), calls=%async_computation.5 | async-start | bytes 5947392 | tf_op jit(solution)/shard_map/all_gather | solution.py:178
  101.4 4.2 %copy-start.1 = (f32[4,320,640]{2,1,0:T(8,128)S(1)}, f32[4,320,640]{2,1,0:T(8,128)}, u32[]{:S(2)}) copy-start(f32[4,320,640]{2,1,0:T(8,128)} %get-tuple-element.224) | copy-start | bytes 9830404 | tf_op jit(solution)/shard_map/while
  110.9 4.2 %copy-start.1 = (f32[4,320,640]{2,1,0:T(8,128)S(1)}, f32[4,320,640]{2,1,0:T(8,128)}, u32[]{:S(2)}) copy-start(f32[4,320,640]{2,1,0:T(8,128)} %get-tuple-element.224) | copy-start | bytes 9830404 | tf_op jit(solution)/shard_map/while
  120.4 4.3 %copy-start.1 = (f32[4,320,640]{2,1,0:T(8,128)S(1)}, f32[4,320,640]{2,1,0:T(8,128)}, u32[]{:S(2)}) copy-start(f32[4,320,640]{2,1,0:T(8,128)} %get-tuple-element.224) | copy-start | bytes 9830404 | tf_op jit(solution)/shard_map/while
  130.0 4.2 %copy-start.1 = (f32[4,320,640]{2,1,0:T(8,128)S(1)}, f32[4,320,640]{2,1,0:T(8,128)}, u32[]{:S(2)}) copy-start(f32[4,320,640]{2,1,0:T(8,128)} %get-tuple-element.224) | copy-start | bytes 9830404 | tf_op jit(solution)/shard_map/while
  139.5 4.3 %copy-start.1 = (f32[4,320,640]{2,1,0:T(8,128)S(1)}, f32[4,320,640]{2,1,0:T(8,128)}, u32[]{:S(2)}) copy-start(f32[4,320,640]{2,1,0:T(8,128)} %get-tuple-element.224) | copy-start | bytes 9830404 | tf_op jit(solution)/shard_map/while
  149.0 4.3 %copy-start.1 = (f32[4,320,640]{2,1,0:T(8,128)S(1)}, f32[4,320,640]{2,1,0:T(8,128)}, u32[]{:S(2)}) copy-start(f32[4,320,640]{2,1,0:T(8,128)} %get-tuple-element.224) | copy-start | bytes 9830404 | tf_op jit(solution)/shard_map/while
  158.6 4.3 %copy-start.1 = (f32[4,320,640]{2,1,0:T(8,128)S(1)}, f32[4,320,640]{2,1,0:T(8,128)}, u32[]{:S(2)}) copy-start(f32[4,320,640]{2,1,0:T(8,128)} %get-tuple-element.224) | copy-start | bytes 9830404 | tf_op jit(solution)/shard_map/while
  168.2 4.3 %copy-start.1 = (f32[4,320,640]{2,1,0:T(8,128)S(1)}, f32[4,320,640]{2,1,0:T(8,128)}, u32[]{:S(2)}) copy-start(f32[4,320,640]{2,1,0:T(8,128)} %get-tuple-element.224) | copy-start | bytes 9830404 | tf_op jit(solution)/shard_map/while
  177.7 4.2 %copy-start.1 = (f32[4,320,640]{2,1,0:T(8,128)S(1)}, f32[4,320,640]{2,1,0:T(8,128)}, u32[]{:S(2)}) copy-start(f32[4,320,640]{2,1,0:T(8,128)} %get-tuple-element.224) | copy-start | bytes 9830404 | tf_op jit(solution)/shard_map/while
  187.2 4.3 %copy-start.1 = (f32[4,320,640]{2,1,0:T(8,128)S(1)}, f32[4,320,640]{2,1,0:T(8,128)}, u32[]{:S(2)}) copy-start(f32[4,320,640]{2,1,0:T(8,128)} %get-tuple-element.224) | copy-start | bytes 9830404 | tf_op jit(solution)/shard_map/while
  196.8 4.2 %copy-start.1 = (f32[4,320,640]{2,1,0:T(8,128)S(1)}, f32[4,320,640]{2,1,0:T(8,128)}, u32[]{:S(2)}) copy-start(f32[4,320,640]{2,1,0:T(8,128)} %get-tuple-element.224) | copy-start | bytes 9830404 | tf_op jit(solution)/shard_map/while
  206.4 4.2 %copy-start.1 = (f32[4,320,640]{2,1,0:T(8,128)S(1)}, f32[4,320,640]{2,1,0:T(8,128)}, u32[]{:S(2)}) copy-start(f32[4,320,640]{2,1,0:T(8,128)} %get-tuple-element.224) | copy-start | bytes 9830404 | tf_op jit(solution)/shard_map/while
  215.9 4.2 %copy-start.1 = (f32[4,320,640]{2,1,0:T(8,128)S(1)}, f32[4,320,640]{2,1,0:T(8,128)}, u32[]{:S(2)}) copy-start(f32[4,320,640]{2,1,0:T(8,128)} %get-tuple-element.224) | copy-start | bytes 9830404 | tf_op jit(solution)/shard_map/while
  225.4 4.2 %copy-start.1 = (f32[4,320,640]{2,1,0:T(8,128)S(1)}, f32[4,320,640]{2,1,0:T(8,128)}, u32[]{:S(2)}) copy-start(f32[4,320,640]{2,1,0:T(8,128)} %get-tuple-element.224) | copy-start | bytes 9830404 | tf_op jit(solution)/shard_map/while
  234.9 4.2 %copy-start.1 = (f32[4,320,640]{2,1,0:T(8,128)S(1)}, f32[4,320,640]{2,1,0:T(8,128)}, u32[]{:S(2)}) copy-start(f32[4,320,640]{2,1,0:T(8,128)} %get-tuple-element.224) | copy-start | bytes 9830404 | tf_op jit(solution)/shard_map/while
  244.4 4.2 %copy-start.1 = (f32[4,320,640]{2,1,0:T(8,128)S(1)}, f32[4,320,640]{2,1,0:T(8,128)}, u32[]{:S(2)}) copy-start(f32[4,320,640]{2,1,0:T(8,128)} %get-tuple-element.224) | copy-start | bytes 9830404 | tf_op jit(solution)/shard_map/while
  251.2 23.9 %copy-start.2 = (f32[2048]{0:T(1024)S(1)}, f32[2048]{0:T(1024)}, u32[]{:S(2)}) copy-start(f32[2048]{0:T(1024)} %param.24) | copy-start | bytes 24580
  251.2 22.5 %all-to-all-start = ((bf16[4,80,2048]{2,1,0:T(8,128)(2,1)}), bf16[4,80,2048]{2,1,0:T(8,128)(2,1)S(1)}, u32[]{:S(2)}, u32[]{:S(2)}) async-start(bf16[4,80,2048]{2,1,0:T(8,128)(2,1)} %bitcast.80), calls=%async_computation | async-start | bytes 2621440 | tf_op jit(solution)/shard_map/all_to_all | solution.py:27
Sparse Core Ops, SparseCore 0:
  9.6 87.3 all-gather.4
  98.9 77.7 all-gather.6
  178.5 70.0 all-gather.8
where the time goes:
time: 343 us; the launch traced here: 341 us
  matrix products  155 us (45%)
  blocking collectives  92.5 us (27%)
  waiting for transfers between devices  43.8 us (13%)
  other arithmetic  27.3 us (8%)
  between operations  13.3 us (4%)
  starting transfers between devices  4.32 us (1%)
  local copies, waits for them, and re-layouts  4.2 us (1%)
    all_gather x1, blocking collectives, local(): rope_piece = lax.all_gather(key_turned, 'sp', axis=0, tiled=True)  52.6 us
    dot_general x16, matrix products, absorb(): jnp.einsum('hqk,khd->qhd', weights.astype(jnp.bfloat16), value_rows, pref...  44.4 us
    dot_general x16, matrix products, absorb(): jnp.einsum('qhd,kd->hqk', query_turned, rope_block, preferred_element_typ...  39 us
    all_gather x1, waiting for transfers between devices, local(): latent_piece = lax.all_gather(latent, 'sp', axis=0, tiled=True)  24.7 us
    dot_general x16, matrix products, absorb(): jnp.dot(latent_block, value_cols, preferred_element_type=jnp.float32)  22.9 us
    dot_general x16, matrix products, absorb(): jnp.dot(latent_block, key_cols, preferred_element_type=jnp.float32)  20.4 us
    all_to_all x1, blocking collectives, sent_to_all(): return lax.all_to_all(copies, axis, split_axis=0, concat_axis=0, tiled=True)  20 us
    all_to_all x1, blocking collectives, summed_on_arrival(): parts = lax.all_to_all(cut_along(array, dim, count), axis, 0, 0, tiled=True)  19.9 us
  transfers between devices with their start and end apart: 4, of which 2 were waited for; matrix products, arithmetic and copies ran while one was open for 50% of the time, Pallas kernels for 0%

commit v1 on v0

v1 whole, which is shorter than its diff:
```python
import math

import jax
import jax.numpy as jnp
import numpy as np
from jax import lax
from jax.experimental import pallas as pl
from jax.experimental.pallas import tpu as pltpu
from jax.sharding import Mesh, PartitionSpec as P


UNROTATED_SIZE = 64
ROPE = 32
VALUE_SIZE = 64
GRID_W = 64
LANES = 128
CORES = 2
BF = jnp.bfloat16
F32 = jnp.float32


NT = (((1,), (1,)), ((), ()))


def shifted(array, axis, step):
    count = lax.axis_size(axis)
    return lax.ppermute(array, axis, [(i, (i + step) % count) for i in range(count)])


def lane_index(shape):
    return lax.broadcasted_iota(jnp.int32, shape, len(shape) - 1)


def prepare_body(at, inverse, lat, gain, key, nope, rope, packed, query, cos_s, sin_s):
    rows = rope.shape[0]
    own = packed.shape[0]
    first = at[0] * rows
    lane = lane_index((rows, LANES))
    position = first + lax.broadcasted_iota(jnp.int32, (rows, LANES), 0)
    place = jnp.where((lane & 16) == 0, position >> int(math.log2(GRID_W)), position & (GRID_W - 1))
    angle = place.astype(F32) * inverse[...]
    cos_s[...] = jnp.cos(angle)
    sin_s[...] = jnp.where((lane & 8) == 0, -1.0, 1.0) * jnp.sin(angle)

    def turn(values, cosine, sine):
        wide = values.astype(F32)
        back = (lane_index(wide.shape) & 8) == 0
        other = jnp.where(back, pltpu.roll(wide, LANES - 8, 1), pltpu.roll(wide, 8, 1))
        return (wide * cosine + other * sine).astype(BF)

    width = nope.shape[1]
    query[:, :width] = nope[...]
    query[:, width:] = turn(rope[...], cos_s[...], sin_s[...])
    mine = pl.ds(pl.multiple_of(at[1] * own, 16), own)
    rank = lat.shape[1]
    wide = lat[...].astype(F32)
    scale = lax.rsqrt(jnp.mean(wide * wide, axis=-1, keepdims=True) + 1e-06)
    packed[:, :rank] = (wide * scale * gain[...]).astype(BF)
    four = jnp.concatenate([key[...]] * (LANES // ROPE), axis=1)
    packed[:, rank:] = turn(four, cos_s[mine, :], sin_s[mine, :])


def attend_body(grp, query_lat, query_rope, near, far, key_w, value_w, out, keys, values, stats):
    step = pl.program_id(0)
    pair = step % 2
    group = grp[step // 2]
    rows = query_lat.shape[1]
    half = near.shape[0]
    rank = key_w.shape[0]
    scale = (UNROTATED_SIZE + ROPE) ** (-0.5) * math.log2(math.e)

    @pl.when(step == 0)
    def _():
        keys[:half, LANES:] = near[:, rank:]
        keys[half:, LANES:] = far[:, rank:]
        values[:, LANES:] = jnp.ones((2 * half, LANES), BF)
        stats[...] = jnp.zeros(stats.shape, F32)

    both = jnp.concatenate([key_w[...], value_w[...]], axis=1)
    for at, source in ((0, near), (half, far)):
        made = jnp.dot(source[:, :rank], both, preferred_element_type=F32).astype(BF)
        keys[at : at + half, :LANES] = made[:, :LANES]
        values[at : at + half, :LANES] = made[:, LANES:]
    lane = lane_index((rows, LANES))
    zero = jnp.zeros((rows, LANES), BF)
    flat = query_lat[0]
    turned = query_rope[0]
    stacked = jnp.concatenate(
        [
            jnp.concatenate(
                [
                    jnp.where(lane // UNROTATED_SIZE == i, flat, zero),
                    jnp.where(lane // ROPE == 2 * pair + i, turned, zero),
                ],
                axis=1,
            )
            for i in range(2)
        ],
        axis=0,
    )
    scores = lax.dot_general(stacked, keys[...], NT, preferred_element_type=F32)
    highest = jnp.max(scores, axis=1, keepdims=True)
    weights = jnp.exp2((scores - highest) * scale).astype(BF)
    summed = jnp.dot(weights, values[...], preferred_element_type=F32)
    totals = summed[:, LANES:]
    mean = summed[:, :LANES] / totals
    out[2 * group + pair] = jnp.where(lane < VALUE_SIZE, mean[:rows], mean[rows:]).astype(BF)
    level = highest * scale + jnp.log2(totals)
    head = 4 * group + 2 * pair
    slot = jnp.where(lane < 48, lane % 16, -1)
    kept = jnp.where(slot == head, level[:rows], stats[...])
    stats[...] = jnp.where(slot == head + 1, level[rows:], kept)

    @pl.when(step == pl.num_programs(0) - 1)
    def _():
        whole = stats[...]
        high = whole.astype(BF)
        rest = whole - high.astype(F32)
        middle = rest.astype(BF)
        low = (rest - middle.astype(F32)).astype(BF)
        out[out.shape[0] - 1] = jnp.where(lane < 16, high, jnp.where(lane < 32, middle, low))


def merge_body(at, p0, p1, p2, p3, w0, w1, w2, w3, residual, gain, mixed, normed):
    parts = (p0, p1, p2, p3)
    rows = p0.shape[1]
    last = p0.shape[0] - 1
    levels = jnp.concatenate([p[last] for p in parts], axis=0)
    slot = lax.broadcasted_iota(jnp.int32, (LANES, LANES), 0)
    column = lane_index((LANES, LANES))
    total = residual[...].astype(F32)
    for k, weight in enumerate((w0, w1, w2, w3)):
        group = lax.rem(at[1] + (4 - k), 4)
        blocks = []
        for pair in range(2):
            head = 4 * group + 2 * pair + column // VALUE_SIZE
            spread = jnp.where((slot < 48) & (slot % 16 == head), 1.0, 0.0).astype(BF)
            wide = jnp.dot(levels, spread, preferred_element_type=F32)
            level = [wide[i * rows : (i + 1) * rows] for i in range(4)]
            top = jnp.maximum(jnp.maximum(level[0], level[1]), jnp.maximum(level[2], level[3]))
            above = jnp.zeros((rows, LANES), F32)
            below = jnp.zeros((rows, LANES), F32)
            for one, part in zip(level, parts):
                share = jnp.exp2(one - top)
                above += share * part[2 * group + pair].astype(F32)
                below += share
            blocks.append((above / below).astype(BF))
        total += jnp.dot(
            jnp.concatenate(blocks, axis=1), weight[...], preferred_element_type=F32
        )
    mixed[...] = total
    norm = lax.rsqrt(jnp.mean(total * total, axis=-1, keepdims=True) + 1e-06)
    normed[...] = (total * norm * gain[...]).astype(BF)


def feed_body(n0, n1, n2, n3, gate_w, up_w, down_w, t0, t1, t2, t3, gate, up, hidden):
    step = pl.program_id(0)
    phases = pl.num_programs(0) // 2
    width = gate_w.shape[-1]

    def flat(ref):
        return ref[...].reshape(-1, width)

    @pl.when(step < phases)
    def _():
        rows = jnp.concatenate([n0[...], n1[...], n2[...], n3[...]], axis=0)
        gate_part = jnp.dot(rows, flat(gate_w), preferred_element_type=F32)
        up_part = jnp.dot(rows, flat(up_w), preferred_element_type=F32)

        @pl.when(step == 0)
        def _():
            gate[...] = gate_part
            up[...] = up_part

        @pl.when(step > 0)
        def _():
            gate[...] += gate_part
            up[...] += up_part

    @pl.when(step == phases - 1)
    def _():
        value = gate[...]
        hidden[...] = (value / (1.0 + jnp.exp(-value)) * up[...]).astype(BF)

    @pl.when(step >= phases)
    def _():
        terms = lax.dot_general(hidden[...], flat(down_w), NT, preferred_element_type=F32)
        terms = terms.astype(BF)
        rows = t0.shape[0]
        for k, ref in enumerate((t0, t1, t2, t3)):
            ref[...] = terms[k * rows : (k + 1) * rows]


def whole(shape):
    return pl.BlockSpec(shape, lambda *_: (0,) * len(shape))


def layer(
    query_nope,
    query_rope,
    token_latent,
    key_rope,
    latent_norm_gain,
    key_expand_weight,
    value_expand_weight,
    residual,
    out_weight,
    ffn_gain,
    gate_weight,
    up_weight,
    down_weight,
):
    rows = query_nope.shape[0]
    members = lax.axis_size("tp")
    own = rows // members
    sp_count = lax.axis_size("z") * CORES
    tp_index = lax.axis_index("tp")
    sp_index = lax.axis_index("z") * CORES + lax.axis_index("core")
    at = jnp.stack([sp_index, tp_index]).astype(jnp.int32)
    rank = token_latent.shape[1]
    nope_width = query_nope.shape[1]
    rope_width = query_rope.shape[1]
    model = residual.shape[1]
    hidden_here = gate_weight.shape[1]
    share = gate_weight.shape[0]

    shards = jnp.concatenate([gate_weight, up_weight, down_weight.T], axis=0)
    gathered = lax.all_gather(shards, ("z", "core"), axis=0, tiled=True)

    freqs = ROPE // 4
    inverse = np.power(10000.0, -np.arange(freqs, dtype=np.float32) / freqs).astype(np.float32)
    inverse = jnp.asarray(np.tile(inverse, LANES // freqs)[None])
    packed, query = pl.pallas_call(
        prepare_body,
        grid_spec=pltpu.PrefetchScalarGridSpec(
            num_scalar_prefetch=1,
            grid=(1,),
            in_specs=[
                whole((1, LANES)),
                pl.BlockSpec((own, rank), lambda s, a: (a[1], 0)),
                whole((1, rank)),
                pl.BlockSpec((own, ROPE), lambda s, a: (a[1], 0)),
                whole((rows, nope_width)),
                whole((rows, rope_width)),
            ],
            out_specs=[whole((own, rank + LANES)), whole((rows, nope_width + rope_width))],
            scratch_shapes=[pltpu.VMEM((rows, LANES), F32), pltpu.VMEM((rows, LANES), F32)],
        ),
        out_shape=[
            jax.ShapeDtypeStruct((own, rank + LANES), BF),
            jax.ShapeDtypeStruct((rows, nope_width + rope_width), BF),
        ],
        name="prepare",
    )(at, inverse, token_latent, latent_norm_gain[None], key_rope, query_nope, query_rope)

    others = [shifted(query, "tp", k) for k in range(1, members)]
    queries = jnp.stack([query] + others)
    near = lax.all_gather(packed, "z", axis=0, tiled=True)
    far = shifted(near, "core", 1)
    outs = [out_weight] + [shifted(out_weight, "tp", k) for k in range(1, members)]

    group_of = lax.rem(tp_index + members - jnp.arange(members), members).astype(jnp.int32)
    keys_here = 2 * near.shape[0]
    blocks = members * nope_width // LANES
    last = blocks - 1

    def now(s):
        return jnp.minimum(s, last)

    attended = pl.pallas_call(
        attend_body,
        grid_spec=pltpu.PrefetchScalarGridSpec(
            num_scalar_prefetch=1,
            grid=(blocks,),
            in_specs=[
                pl.BlockSpec((1, rows, LANES), lambda s, g: (now(s) // 2, 0, now(s) % 2)),
                pl.BlockSpec((1, rows, LANES), lambda s, g: (now(s) // 2, 0, nope_width // LANES)),
                whole(near.shape),
                whole(near.shape),
                pl.BlockSpec((rank, LANES), lambda s, g: (0, 2 * g[now(s) // 2] + now(s) % 2)),
                pl.BlockSpec((rank, LANES), lambda s, g: (0, 2 * g[now(s) // 2] + now(s) % 2)),
            ],
            out_specs=whole((blocks + 1, rows, LANES)),
            scratch_shapes=[
                pltpu.VMEM((keys_here, 2 * LANES), BF),
                pltpu.VMEM((keys_here, 2 * LANES), BF),
                pltpu.VMEM((rows, LANES), F32),
            ],
        ),
        out_shape=jax.ShapeDtypeStruct((blocks + 1, rows, LANES), BF),
        name="attend",
    )(group_of, queries, queries, near, far, key_expand_weight, value_expand_weight)

    def block_for(step):
        where = lax.rem(tp_index + step, members) * own
        return lax.dynamic_slice_in_dim(attended, where, own, 1)

    parts = [block_for(0)] + [shifted(block_for(k), "tp", k) for k in range(1, members)]
    mixed, normed = pl.pallas_call(
        merge_body,
        grid_spec=pltpu.PrefetchScalarGridSpec(
            num_scalar_prefetch=1,
            grid=(1,),
            in_specs=[whole((blocks + 1, own, LANES))] * members
            + [whole(out_weight.shape)] * members
            + [pl.BlockSpec((own, model), lambda s, a: (a[1], 0)), whole((1, model))],
            out_specs=[whole((own, model)), whole((own, model))],
        ),
        out_shape=[
            jax.ShapeDtypeStruct((own, model), F32),
            jax.ShapeDtypeStruct((own, model), BF),
        ],
        name="merge",
    )(at, *parts, *outs, residual, ffn_gain[None])
    rows_in = [normed] + [shifted(normed, "tp", k) for k in range(1, members)]

    phases = 4
    cut = model // phases
    weights = gathered.reshape(phases, sp_count // phases, 3, share, hidden_here)

    def weight_spec(kind):
        first = kind < 2

        def index(s):
            chunk = jnp.minimum(s, phases - 1) if first else jnp.maximum(s - phases, 0)
            return (chunk, 0, kind, 0, 0)

        return pl.BlockSpec((1, sp_count // phases, 1, share, hidden_here), index)

    terms = pl.pallas_call(
        feed_body,
        grid=(2 * phases,),
        in_specs=[pl.BlockSpec((own, cut), lambda s: (0, jnp.minimum(s, phases - 1)))] * members
        + [weight_spec(kind) for kind in range(3)],
        out_specs=[pl.BlockSpec((own, cut), lambda s: (0, jnp.maximum(s - phases, 0)))] * members,
        out_shape=[jax.ShapeDtypeStruct((own, model), BF)] * members,
        scratch_shapes=[
            pltpu.VMEM((rows, hidden_here), F32),
            pltpu.VMEM((rows, hidden_here), F32),
            pltpu.VMEM((rows, hidden_here), BF),
        ],
        name="feed",
    )(*rows_in, weights, weights, weights)
    arrived = [terms[0]] + [shifted(terms[k], "tp", -k) for k in range(1, members)]
    result = mixed
    for one in arrived:
        result = result + one.astype(F32)
    return result.astype(BF)


def solution(mesh):
    groups, sp_count, members = mesh.devices.shape
    finer = Mesh(
        mesh.devices.reshape(groups, sp_count // CORES, CORES, members),
        ("grp", "z", "core", "tp"),
    )
    tokens = ("grp", "z", "core")
    return jax.shard_map(
        layer,
        mesh=finer,
        in_specs=(
            P(tokens, "tp"),
            P(tokens, "tp"),
            P(tokens, None),
            P(tokens, None),
            P(),
            P(),
            P(),
            P(tokens, None),
            P("tp", None),
            P(),
            P(("z", "core"), "tp"),
            P(("z", "core"), "tp"),
            P("tp", ("z", "core")),
        ),
        out_specs=P(tokens + ("tp",), None),
        check_vma=False,
    )
```

time: 343 us -> 270 us (0.79)
  the two profiles are of different devices: /device:TPU:40 before, /device:TPU:33 now
where the time goes in v1:
time: 270 us
  waiting for transfers between devices  97.6 us (36%)
  blocking collectives  60.5 us (22%)
  Pallas kernels  59.7 us (22%)
  starting transfers between devices  26.7 us (10%)
  between operations  13.5 us (5%)
  other arithmetic  7.36 us (3%)
  local copies, waits for them, and re-layouts  4.17 us (2%)
    ppermute x16, waiting for transfers between devices, shifted(): lax.ppermute(array, axis, [(i, (i + step) % count) for i in range(count)])  97.5 us
    all_gather x1, blocking collectives, layer(): near = lax.all_gather(packed, 'z', axis=0, tiled=True)  60.5 us
    pallas_call x1, Pallas kernels, layer(): pl.pallas_call(attend_body, grid_spec=pltpu.PrefetchScalarGridSpec(num_sc...  36.1 us
    ppermute x16, starting transfers between devices, shifted(): lax.ppermute(array, axis, [(i, (i + step) % count) for i in range(count)])  26.7 us
    pallas_call x1, Pallas kernels, layer(): pl.pallas_call(feed_body, grid=(2 * phases,), in_specs=[pl.BlockSpec((own...  14.7 us
    pallas_call x1, Pallas kernels, layer(): pl.pallas_call(merge_body, grid_spec=pltpu.PrefetchScalarGridSpec(num_sca...  5.82 us
  transfers between devices with their start and end apart: 17, of which 11 were waited for; matrix products, arithmetic and copies ran while one was open for 2% of the time, Pallas kernels for 17%

profile of v1, /device:TPU:33, one launch (start us, length us, event | category | flops | bytes accessed | tf_op | source)
XLA Modules:
  0.0 269.6 jit_solution(15194850182865733707)
XLA Ops:
  6.6 2.0 pad_maximum_fusion.1
  8.6 0.7 copy.15.key
  10.0 3.1 %prepare.1 = (bf16[80,384]{1,0:T(8,128)(2,1)}, bf16[320,384]{1,0:T(8,128)(2,1)}) custom-call(s32[2]{0:T(128)} %pad_add_fusion.at, f32[1,128]{1,0:T(1,128)} %constant.41.clone.inverse, bf16[320,256]{1,0:T(8,128)(2,1)} %lat.1, f32[1,256]{1,0:T(1,128)} %bitcast.16, bf16[320,32]{1,0:T(8,128)(2,1)} %copy.15.key, bf16[320,256]{1,0:T(8,128)(2,1)} %nope.1, ...), custom_call_target="tpu_custom_call" | custom-call | tf_op jit(solution)/shard_map/prepare/pallas_call | solution.py:233
  13.1 60.5 %all_gather.6.near = bf16[1280,384]{1,0:T(8,128)(2,1)S(1)} all-gather(bf16[80,384]{1,0:T(8,128)(2,1)} %get-tuple-element.14), channel_id=1, replica_groups=mesh['grp'=2,'z'=16,'core'=2,'tp'=4] {'z'}, dimensions={0}, use_global_device_ids=true | all-gather | bytes 1044480 | tf_op jit(solution)/shard_map/all_gather | solution.py:258
  73.6 7.4 %collective-permute-start.3 = (bf16[1280,384]{1,0:T(8,128)(2,1)S(1)}, bf16[1280,384]{1,0:T(8,128)(2,1)}, u32[]{:S(2)}, u32[]{:S(2)}) collective-permute-start(bf16[1280,384]{1,0:T(8,128)(2,1)S(1)} %all_gather.6.near), channel_id=1, source_target_pairs={{0,4},{4,0},{1,5},{5,1},{2,6},{6,2},{3,7},{7,3},{8,12},{12,8},{9,1... | collective-permute-start | bytes 2949128 | tf_op jit(solution)/shard_map/ppermute | solution.py:27
  81.0 2.0 collective-permute-start.7
  83.0 0.8 collective-permute-start
  83.8 1.3 collective-permute-start.8
  85.1 2.1 collective-permute-start.9
  87.2 25.5 %collective-permute-done = bf16[320,384]{1,0:T(8,128)(2,1)} collective-permute-done((bf16[320,384]{1,0:T(8,128)(2,1)}, bf16[320,384]{1,0:T(8,128)(2,1)}, u32[]{:S(2)}, u32[]{:S(2)}) %collective-permute-start) | collective-permute-done | bytes 245792 | tf_op jit(solution)/shard_map/ppermute | solution.py:27
  112.7 1.4 collective-permute-start.1
  114.1 27.2 %collective-permute-done.1 = bf16[320,384]{1,0:T(8,128)(2,1)} collective-permute-done((bf16[320,384]{1,0:T(8,128)(2,1)}, bf16[320,384]{1,0:T(8,128)(2,1)}, u32[]{:S(2)}, u32[]{:S(2)}) %collective-permute-start.1) | collective-permute-done | bytes 245792 | tf_op jit(solution)/shard_map/ppermute | solution.py:27
  141.9 6.3 %collective-permute-done.2 = bf16[320,384]{1,0:T(8,128)(2,1)} collective-permute-done((bf16[320,384]{1,0:T(8,128)(2,1)}, bf16[320,384]{1,0:T(8,128)(2,1)}, u32[]{:S(2)}, u32[]{:S(2)}) %collective-permute-start.2) | collective-permute-done | bytes 245792 | tf_op jit(solution)/shard_map/ppermute | solution.py:27
  148.2 2.3 pad_maximum_fusion.query_lat.query_rope
  150.5 36.1 %attend.1 = bf16[9,320,128]{2,1,0:T(8,128)(2,1)} custom-call(s32[4]{0:T(128)} %compare_select_fusion.grp, bf16[4,320,384]{2,1,0:T(8,128)(2,1)} %pad_maximum_fusion.query_lat.query_rope, bf16[4,320,384]{2,1,0:T(8,128)(2,1)} %pad_maximum_fusion.query_lat.query_rope, bf16[1280,384]{1,0:T(8,128)(2,1)} %copy-done, bf16[1280,384]{1,0:T(8,128)(2,1)} %collective-permute-done.3.far, ...), custom_call_target="tpu_custom_call" | custom-call | tf_op jit(solution)/shard_map/attend/pallas_call | solution.py:270
  186.6 2.0 constant_dynamic-slice_fusion
  188.6 2.7 collective-permute-start.5
  191.5 2.7 collective-permute-done.4.p1
  194.2 3.9 %collective-permute-done.5.p2 = bf16[9,80,128]{2,1,0:T(8,128)(2,1)S(1)} collective-permute-done((bf16[9,80,128]{2,1,0:T(8,128)(2,1)S(1)}, bf16[9,80,128]{2,1,0:T(8,128)(2,1)S(1)}, u32[]{:S(2)}, u32[]{:S(2)}) %collective-permute-start.5) | collective-permute-done | bytes 184352 | tf_op jit(solution)/shard_map/ppermute | solution.py:27
  198.1 0.9 collective-permute-done.6.p3
  199.0 0.7 copy-done.10
  199.7 5.8 %merge.1 = (f32[80,2048]{1,0:T(8,128)}, bf16[80,2048]{1,0:T(8,128)(2,1)}) custom-call(s32[2]{0:T(128)} %pad_add_fusion.at, bf16[9,80,128]{2,1,0:T(8,128)(2,1)} %get-tuple-element.24.p0, bf16[9,80,128]{2,1,0:T(8,128)(2,1)} %copy-done.8, bf16[9,80,128]{2,1,0:T(8,128)(2,1)} %copy-done.9, bf16[9,80,128]{2,1,0:T(8,128)(2,1)} %copy-done.10, bf16[256,2048]{1,0:T(8,128)(2,1)} %w0.1, ...), custom_call_target="tpu_custom_call" | custom-call | tf_op jit(solution)/shard_map/merge/pallas_call | solution.py:299
  205.5 0.9 collective-permute-start.10
  206.4 3.9 %collective-permute-start.11 = (bf16[80,2048]{1,0:T(8,128)(2,1)}, bf16[80,2048]{1,0:T(8,128)(2,1)S(1)}, u32[]{:S(2)}, u32[]{:S(2)}) collective-permute-start(bf16[80,2048]{1,0:T(8,128)(2,1)} %get-tuple-element.16.n0), channel_id=1, source_target_pairs={{0,2},{1,3},{2,0},{3,1},{4,6},{5,7},{6,4},{7,5},{8,10},{9,11},{10,... | collective-permute-start | bytes 983048 | tf_op jit(solution)/shard_map/ppermute | solution.py:27
  210.2 5.3 %collective-permute-done.10.n1 = bf16[80,2048]{1,0:T(8,128)(2,1)S(1)} collective-permute-done((bf16[80,2048]{1,0:T(8,128)(2,1)}, bf16[80,2048]{1,0:T(8,128)(2,1)S(1)}, u32[]{:S(2)}, u32[]{:S(2)}) %collective-permute-start.10) | collective-permute-done | bytes 327712 | tf_op jit(solution)/shard_map/ppermute | solution.py:27
  215.6 8.6 %collective-permute-done.11.n2 = bf16[80,2048]{1,0:T(8,128)(2,1)S(1)} collective-permute-done((bf16[80,2048]{1,0:T(8,128)(2,1)}, bf16[80,2048]{1,0:T(8,128)(2,1)S(1)}, u32[]{:S(2)}, u32[]{:S(2)}) %collective-permute-start.11) | collective-permute-done | bytes 327712 | tf_op jit(solution)/shard_map/ppermute | solution.py:27
  225.0 14.7 %feed.1 = (bf16[80,2048]{1,0:T(8,128)(2,1)}, bf16[80,2048]{1,0:T(8,128)(2,1)}, bf16[80,2048]{1,0:T(8,128)(2,1)}, bf16[80,2048]{1,0:T(8,128)(2,1)}) custom-call(bf16[80,2048]{1,0:T(8,128)(2,1)} %get-tuple-element.16.n0, bf16[80,2048]{1,0:T(8,128)(2,1)} %copy-done.4, bf16[80,2048]{1,0:T(8,128)(2,1)} %copy-done.5, bf16[80,2048]{1,0:T(8,128)(2,1)} %copy-done.6, ...), custom_call_target="tpu_custom_call" | custom-call | tf_op jit(solution)/shard_map/feed/pallas_call | solution.py:330
  239.7 3.3 %collective-permute-start.13 = (bf16[80,2048]{1,0:T(8,128)(2,1)}, bf16[80,2048]{1,0:T(8,128)(2,1)S(1)}, u32[]{:S(2)}, u32[]{:S(2)}) collective-permute-start(bf16[80,2048]{1,0:T(8,128)(2,1)} %get-tuple-element.18), channel_id=1, source_target_pairs={{0,3},{1,0},{2,1},{3,2},{4,7},{5,4},{6,5},{7,6},{8,11},{9,8},{10,9... | collective-permute-start | bytes 983048 | tf_op jit(solution)/shard_map/ppermute | solution.py:27
  243.0 0.7 collective-permute-start.15
  243.7 13.0 %collective-permute-done.13 = bf16[80,2048]{1,0:T(8,128)(2,1)S(1)} collective-permute-done((bf16[80,2048]{1,0:T(8,128)(2,1)}, bf16[80,2048]{1,0:T(8,128)(2,1)S(1)}, u32[]{:S(2)}, u32[]{:S(2)}) %collective-permute-start.13) | collective-permute-done | bytes 327712 | tf_op jit(solution)/shard_map/ppermute | solution.py:27
  256.8 4.0 %collective-permute-done.15 = bf16[80,2048]{1,0:T(8,128)(2,1)S(1)} collective-permute-done((bf16[80,2048]{1,0:T(8,128)(2,1)}, bf16[80,2048]{1,0:T(8,128)(2,1)S(1)}, u32[]{:S(2)}, u32[]{:S(2)}) %collective-permute-start.15) | collective-permute-done | bytes 327712 | tf_op jit(solution)/shard_map/ppermute | solution.py:27
  260.8 1.9 add_convert_fusion
  (39 shorter events, 2.4 us)
Async XLA Ops:
  6.5 2.0 copy-start.11
  6.5 217.6 %all-gather.2.cloned.1.call-start = ((), (), s32[]{:S(2)}) async-start(), calls=%async_computation | async-start | bytes 17842176 | tf_op jit(solution)/shard_map/all_gather | solution.py:228
  8.5 72.5 %copy-start.1 = (bf16[256,2048]{1,0:T(8,128)(2,1)S(1)}, bf16[256,2048]{1,0:T(8,128)(2,1)}, u32[]{:S(2)}) copy-start(bf16[256,2048]{1,0:T(8,128)(2,1)} %w0.1) | copy-start | bytes 3145732
  13.1 135.1 %copy-start.7 = (bf16[320,384]{1,0:T(8,128)(2,1)S(1)}, bf16[320,384]{1,0:T(8,128)(2,1)}, u32[]{:S(2)}) copy-start(bf16[320,384]{1,0:T(8,128)(2,1)} %get-tuple-element.13) | copy-start | bytes 737284
  73.6 76.9 %copy-start = (bf16[1280,384]{1,0:T(8,128)(2,1)}, bf16[1280,384]{1,0:T(8,128)(2,1)S(1)}, u32[]{:S(2)}) copy-start(bf16[1280,384]{1,0:T(8,128)(2,1)S(1)} %all_gather.6.near) | copy-start | bytes 2949124
  73.6 76.9 %collective-permute-start.3 = (bf16[1280,384]{1,0:T(8,128)(2,1)S(1)}, bf16[1280,384]{1,0:T(8,128)(2,1)}, u32[]{:S(2)}, u32[]{:S(2)}) collective-permute-start(bf16[1280,384]{1,0:T(8,128)(2,1)S(1)} %all_gather.6.near), channel_id=1, source_target_pairs={{0,4},{4,0},{1,5},{5,1},{2,6},{6,2},{3,7},{7,3},{8,12},{12,8},{9,1... | collective-permute-start | bytes 2949128 | tf_op jit(solution)/shard_map/ppermute | solution.py:27
  81.0 110.3 %collective-permute-start.7 = (bf16[256,2048]{1,0:T(8,128)(2,1)S(1)}, bf16[256,2048]{1,0:T(8,128)(2,1)S(1)}, u32[]{:S(2)}, u32[]{:S(2)}) collective-permute-start(bf16[256,2048]{1,0:T(8,128)(2,1)S(1)} %copy-done.1), channel_id=1, source_target_pairs={{0,1},{1,2},{2,3},{3,0},{4,5},{5,6},{6,7},{7,4},{8,9},{9,10},{10,1... | collective-permute-start | bytes 3145736 | tf_op jit(solution)/shard_map/ppermute | solution.py:27
  83.0 29.7 %collective-permute-start = (bf16[320,384]{1,0:T(8,128)(2,1)}, bf16[320,384]{1,0:T(8,128)(2,1)}, u32[]{:S(2)}, u32[]{:S(2)}) collective-permute-start(bf16[320,384]{1,0:T(8,128)(2,1)} %get-tuple-element.13), channel_id=1, source_target_pairs={{0,1},{1,2},{2,3},{3,0},{4,5},{5,6},{6,7},{7,4},{8,9},{9,10},{10,1... | collective-permute-start | bytes 737288 | tf_op jit(solution)/shard_map/ppermute | solution.py:27
  83.8 107.7 %collective-permute-start.8 = (bf16[256,2048]{1,0:T(8,128)(2,1)S(1)}, bf16[256,2048]{1,0:T(8,128)(2,1)}, u32[]{:S(2)}, u32[]{:S(2)}) collective-permute-start(bf16[256,2048]{1,0:T(8,128)(2,1)S(1)} %copy-done.1), channel_id=1, source_target_pairs={{0,2},{1,3},{2,0},{3,1},{4,6},{5,7},{6,4},{7,5},{8,10},{9,11},{10,... | collective-permute-start | bytes 3145736 | tf_op jit(solution)/shard_map/ppermute | solution.py:27
  85.1 106.4 %collective-permute-start.9 = (bf16[256,2048]{1,0:T(8,128)(2,1)S(1)}, bf16[256,2048]{1,0:T(8,128)(2,1)}, u32[]{:S(2)}, u32[]{:S(2)}) collective-permute-start(bf16[256,2048]{1,0:T(8,128)(2,1)S(1)} %copy-done.1), channel_id=1, source_target_pairs={{0,3},{1,0},{2,1},{3,2},{4,7},{5,4},{6,5},{7,6},{8,11},{9,8},{10,9... | collective-permute-start | bytes 3145736 | tf_op jit(solution)/shard_map/ppermute | solution.py:27
  112.7 28.7 %collective-permute-start.1 = (bf16[320,384]{1,0:T(8,128)(2,1)}, bf16[320,384]{1,0:T(8,128)(2,1)}, u32[]{:S(2)}, u32[]{:S(2)}) collective-permute-start(bf16[320,384]{1,0:T(8,128)(2,1)} %get-tuple-element.13), channel_id=1, source_target_pairs={{0,2},{1,3},{2,0},{3,1},{4,6},{5,7},{6,4},{7,5},{8,10},{9,11},{10,... | collective-permute-start | bytes 737288 | tf_op jit(solution)/shard_map/ppermute | solution.py:27
  141.3 6.9 %collective-permute-start.2 = (bf16[320,384]{1,0:T(8,128)(2,1)}, bf16[320,384]{1,0:T(8,128)(2,1)}, u32[]{:S(2)}, u32[]{:S(2)}) collective-permute-start(bf16[320,384]{1,0:T(8,128)(2,1)} %get-tuple-element.13), channel_id=1, source_target_pairs={{0,3},{1,0},{2,1},{3,2},{4,7},{5,4},{6,5},{7,6},{8,11},{9,8},{10,9... | collective-permute-start | bytes 737288 | tf_op jit(solution)/shard_map/ppermute | solution.py:27
  188.6 5.6 %collective-permute-start.4 = (bf16[9,80,128]{2,1,0:T(8,128)(2,1)S(1)}, bf16[9,80,128]{2,1,0:T(8,128)(2,1)S(1)}, u32[]{:S(2)}, u32[]{:S(2)}) collective-permute-start(bf16[9,80,128]{2,1,0:T(8,128)(2,1)S(1)} %get-tuple-element.23), channel_id=1, source_target_pairs={{0,1},{1,2},{2,3},{3,0},{4,5},{5,6},{6,7},{7,4},{8,9},{9,10},{10,1... | collective-permute-start | bytes 552968 | tf_op jit(solution)/shard_map/ppermute | solution.py:27
  188.6 9.5 %collective-permute-start.5 = (bf16[9,80,128]{2,1,0:T(8,128)(2,1)S(1)}, bf16[9,80,128]{2,1,0:T(8,128)(2,1)S(1)}, u32[]{:S(2)}, u32[]{:S(2)}) collective-permute-start(bf16[9,80,128]{2,1,0:T(8,128)(2,1)S(1)} %get-tuple-element.22), channel_id=1, source_target_pairs={{0,2},{1,3},{2,0},{3,1},{4,6},{5,7},{6,4},{7,5},{8,10},{9,11},{10,... | collective-permute-start | bytes 552968 | tf_op jit(solution)/shard_map/ppermute | solution.py:27
  191.2 7.8 %copy-start.2 = (bf16[256,2048]{1,0:T(8,128)(2,1)}, bf16[256,2048]{1,0:T(8,128)(2,1)S(1)}, u32[]{:S(2)}) copy-start(bf16[256,2048]{1,0:T(8,128)(2,1)S(1)} %collective-permute-done.7.w1) | copy-start | bytes 3145732
  191.2 7.8 %collective-permute-start.6 = (bf16[9,80,128]{2,1,0:T(8,128)(2,1)S(1)}, bf16[9,80,128]{2,1,0:T(8,128)(2,1)S(1)}, u32[]{:S(2)}, u32[]{:S(2)}) collective-permute-start(bf16[9,80,128]{2,1,0:T(8,128)(2,1)S(1)} %get-tuple-element.21), channel_id=1, source_target_pairs={{0,3},{1,0},{2,1},{3,2},{4,7},{5,4},{6,5},{7,6},{8,11},{9,8},{10,9... | collective-permute-start | bytes 552968 | tf_op jit(solution)/shard_map/ppermute | solution.py:27
  194.2 4.8 %copy-start.8 = (bf16[9,80,128]{2,1,0:T(8,128)(2,1)}, bf16[9,80,128]{2,1,0:T(8,128)(2,1)S(1)}, u32[]{:S(2)}) copy-start(bf16[9,80,128]{2,1,0:T(8,128)(2,1)S(1)} %collective-permute-done.4.p1) | copy-start | bytes 552964
  198.1 0.9 copy-start.9
  199.0 0.7 copy-start.10
  205.5 10.0 %collective-permute-start.10 = (bf16[80,2048]{1,0:T(8,128)(2,1)}, bf16[80,2048]{1,0:T(8,128)(2,1)S(1)}, u32[]{:S(2)}, u32[]{:S(2)}) collective-permute-start(bf16[80,2048]{1,0:T(8,128)(2,1)} %get-tuple-element.16.n0), channel_id=1, source_target_pairs={{0,1},{1,2},{2,3},{3,0},{4,5},{5,6},{6,7},{7,4},{8,9},{9,10},{10,1... | collective-permute-start | bytes 983048 | tf_op jit(solution)/shard_map/ppermute | solution.py:27
  206.4 17.8 %collective-permute-start.11 = (bf16[80,2048]{1,0:T(8,128)(2,1)}, bf16[80,2048]{1,0:T(8,128)(2,1)S(1)}, u32[]{:S(2)}, u32[]{:S(2)}) collective-permute-start(bf16[80,2048]{1,0:T(8,128)(2,1)} %get-tuple-element.16.n0), channel_id=1, source_target_pairs={{0,2},{1,3},{2,0},{3,1},{4,6},{5,7},{6,4},{7,5},{8,10},{9,11},{10,... | collective-permute-start | bytes 983048 | tf_op jit(solution)/shard_map/ppermute | solution.py:27
  210.2 13.9 %collective-permute-start.12 = (bf16[80,2048]{1,0:T(8,128)(2,1)}, bf16[80,2048]{1,0:T(8,128)(2,1)S(1)}, u32[]{:S(2)}, u32[]{:S(2)}) collective-permute-start(bf16[80,2048]{1,0:T(8,128)(2,1)} %get-tuple-element.16.n0), channel_id=1, source_target_pairs={{0,3},{1,0},{2,1},{3,2},{4,7},{5,4},{6,5},{7,6},{8,11},{9,8},{10,9... | collective-permute-start | bytes 983048 | tf_op jit(solution)/shard_map/ppermute | solution.py:27
  215.5 8.6 %copy-start.4 = (bf16[80,2048]{1,0:T(8,128)(2,1)}, bf16[80,2048]{1,0:T(8,128)(2,1)S(1)}, u32[]{:S(2)}) copy-start(bf16[80,2048]{1,0:T(8,128)(2,1)S(1)} %collective-permute-done.10.n1) | copy-start | bytes 983044
  224.1 0.7 copy-start.5
  224.2 0.8 copy-start.6
  225.0 35.8 %copy-start.3 = (f32[80,2048]{1,0:T(8,128)S(1)}, f32[80,2048]{1,0:T(8,128)}, u32[]{:S(2)}) copy-start(f32[80,2048]{1,0:T(8,128)} %get-tuple-element.15) | copy-start | bytes 1966084
  239.7 17.1 %collective-permute-start.13 = (bf16[80,2048]{1,0:T(8,128)(2,1)}, bf16[80,2048]{1,0:T(8,128)(2,1)S(1)}, u32[]{:S(2)}, u32[]{:S(2)}) collective-permute-start(bf16[80,2048]{1,0:T(8,128)(2,1)} %get-tuple-element.18), channel_id=1, source_target_pairs={{0,3},{1,0},{2,1},{3,2},{4,7},{5,4},{6,5},{7,6},{8,11},{9,8},{10,9... | collective-permute-start | bytes 983048 | tf_op jit(solution)/shard_map/ppermute | solution.py:27
  243.0 13.8 %collective-permute-start.14 = (bf16[80,2048]{1,0:T(8,128)(2,1)}, bf16[80,2048]{1,0:T(8,128)(2,1)S(1)}, u32[]{:S(2)}, u32[]{:S(2)}) collective-permute-start(bf16[80,2048]{1,0:T(8,128)(2,1)} %get-tuple-element.19), channel_id=1, source_target_pairs={{0,2},{1,3},{2,0},{3,1},{4,6},{5,7},{6,4},{7,5},{8,10},{9,11},{10,... | collective-permute-start | bytes 983048 | tf_op jit(solution)/shard_map/ppermute | solution.py:27
  243.0 17.8 %collective-permute-start.15 = (bf16[80,2048]{1,0:T(8,128)(2,1)}, bf16[80,2048]{1,0:T(8,128)(2,1)S(1)}, u32[]{:S(2)}, u32[]{:S(2)}) collective-permute-start(bf16[80,2048]{1,0:T(8,128)(2,1)} %get-tuple-element.20), channel_id=1, source_target_pairs={{0,1},{1,2},{2,3},{3,0},{4,5},{5,6},{6,7},{7,4},{8,9},{9,10},{10,1... | collective-permute-start | bytes 983048 | tf_op jit(solution)/shard_map/ppermute | solution.py:27
Sparse Core Ops, SparseCore 0:
  9.2 131.3 all-gather.1

commit v2 on v1

v2 whole, which is shorter than its diff:
```python
import math

import jax
import jax.numpy as jnp
import numpy as np
from jax import lax
from jax.experimental import pallas as pl
from jax.experimental.pallas import tpu as pltpu
from jax.sharding import Mesh, PartitionSpec as P


UNROTATED_SIZE = 64
ROPE = 32
VALUE_SIZE = 64
GRID_W = 64
LANES = 128
CORES = 2
BF = jnp.bfloat16
F32 = jnp.float32


NT = (((1,), (1,)), ((), ()))


def shifted(array, axis, step):
    count = lax.axis_size(axis)
    return lax.ppermute(array, axis, [(i, (i + step) % count) for i in range(count)])


def lane_index(shape):
    return lax.broadcasted_iota(jnp.int32, shape, len(shape) - 1)


def prepare_body(at, inverse, lat, gain, key, nope, rope, packed, query, cos_s, sin_s):
    rows = rope.shape[0]
    own = packed.shape[0]
    first = at[0] * rows
    lane = lane_index((rows, LANES))
    position = first + lax.broadcasted_iota(jnp.int32, (rows, LANES), 0)
    place = jnp.where((lane & 16) == 0, position >> int(math.log2(GRID_W)), position & (GRID_W - 1))
    angle = place.astype(F32) * inverse[...]
    cos_s[...] = jnp.cos(angle)
    sin_s[...] = jnp.where((lane & 8) == 0, -1.0, 1.0) * jnp.sin(angle)

    def turn(values, cosine, sine):
        wide = values.astype(F32)
        back = (lane_index(wide.shape) & 8) == 0
        other = jnp.where(back, pltpu.roll(wide, LANES - 8, 1), pltpu.roll(wide, 8, 1))
        return (wide * cosine + other * sine).astype(BF)

    width = nope.shape[1]
    query[:, :width] = nope[...]
    query[:, width:] = turn(rope[...], cos_s[...], sin_s[...])
    mine = pl.ds(pl.multiple_of(at[1] * own, 16), own)
    rank = lat.shape[1]
    wide = lat[...].astype(F32)
    scale = lax.rsqrt(jnp.mean(wide * wide, axis=-1, keepdims=True) + 1e-06)
    packed[:, :rank] = (wide * scale * gain[...]).astype(BF)
    four = jnp.concatenate([key[...]] * (LANES // ROPE), axis=1)
    packed[:, rank:] = turn(four, cos_s[mine, :], sin_s[mine, :])


def attend_body(
    at, q0, q1, q2, q3, near, far, key_w, value_w, o0, o1, o2, o3, held, stacked, values, scores, highest, stats
):
    step = pl.program_id(0)
    last = pl.num_programs(0) - 1
    turn = step // 2
    pair = step % 2
    group = lax.rem(at[1] + 4 - turn, 4)
    rows = q0.shape[0]
    own = o0.shape[1]
    half = near.shape[0]
    rank = key_w.shape[0]
    scale = (UNROTATED_SIZE + ROPE) ** (-0.5) * math.log2(math.e)
    tile = 256
    wide = 2 * tile
    chunks = 2 * half // wide
    lane = lane_index((rows, LANES))

    @pl.when(step == 0)
    def _():
        values[:, LANES:] = jnp.ones((2 * half, LANES), BF)
        stats[...] = jnp.zeros(stats.shape, F32)

    zero = jnp.zeros((rows, LANES), BF)
    for k, query in enumerate((q0, q1, q2, q3)):
        for p in range(2):

            @pl.when(step == 2 * k + p)
            def _():
                flat = query[:, p * LANES : (p + 1) * LANES]
                turned = query[:, 2 * LANES :]
                for i in range(2):
                    mine = slice(i * rows, (i + 1) * rows)
                    stacked[mine, :LANES] = jnp.where(lane // UNROTATED_SIZE == i, flat, zero)
                    stacked[mine, LANES:] = jnp.where(lane // ROPE == 2 * p + i, turned, zero)

    both = jnp.concatenate([key_w[...], value_w[...]], axis=1)
    asked = stacked[...]
    for c in range(chunks):
        top = None
        for u in (c, c + chunks):
            source, from_row = (near, u * tile) if u < chunks else (far, u * tile - half)
            made = jnp.dot(
                source[from_row : from_row + tile, :rank], both, preferred_element_type=F32
            ).astype(BF)
            values[u * tile : (u + 1) * tile, :LANES] = made[:, LANES:]
            keys = jnp.concatenate([made[:, :LANES], source[from_row : from_row + tile, rank:]], axis=1)
            part = lax.dot_general(asked, keys, NT, preferred_element_type=F32)
            scores[:, u * tile : (u + 1) * tile] = part
            level = jnp.maximum(part[:, :LANES], part[:, LANES:])
            top = level if top is None else jnp.maximum(top, level)
        highest[...] = top if c == 0 else jnp.maximum(highest[...], top)

    @pl.when(step <= last)
    def _():
        peak = jnp.broadcast_to(jnp.max(highest[...], axis=1, keepdims=True), (2 * rows, LANES))
        many = jnp.concatenate([peak] * (wide // LANES), axis=1)
        summed = None
        for c in range(chunks):
            spot = slice(c * wide, (c + 1) * wide)
            weights = jnp.exp2((scores[:, spot] - many) * scale).astype(BF)
            more = jnp.dot(weights, values[spot, :], preferred_element_type=F32)
            summed = more if c == 0 else summed + more
        totals = summed[:, LANES:]
        mean = summed[:, :LANES] / totals
        held[2 * group + pair] = jnp.where(lane < VALUE_SIZE, mean[:rows], mean[rows:]).astype(BF)
        level = peak * scale + jnp.log2(totals)
        head = 4 * group + 2 * pair
        place = jnp.where(lane < 48, lane % 16, -1)
        kept = jnp.where(place == head, level[:rows], stats[...])
        stats[...] = jnp.where(place == head + 1, level[rows:], kept)

    @pl.when(step == last)
    def _():
        every = stats[...]
        high = every.astype(BF)
        rest = every - high.astype(F32)
        middle = rest.astype(BF)
        low = (rest - middle.astype(F32)).astype(BF)
        held[held.shape[0] - 1] = jnp.where(lane < 16, high, jnp.where(lane < 32, middle, low))
        for k, ref in enumerate((o0, o1, o2, o3)):
            start = pl.multiple_of(lax.rem(at[1] + k, 4) * own, 16)
            ref[...] = held[:, pl.ds(start, own), :]


def merge_body(at, p0, p1, p2, p3, w0, w1, w2, w3, residual, gain, mixed, normed_a, normed_b):
    parts = (p0, p1, p2, p3)
    rows = p0.shape[1]
    last = p0.shape[0] - 1
    levels = jnp.concatenate([p[last] for p in parts], axis=0)
    slot = lax.broadcasted_iota(jnp.int32, (LANES, LANES), 0)
    column = lane_index((LANES, LANES))
    total = residual[...].astype(F32)
    for k, weight in enumerate((w0, w1, w2, w3)):
        group = lax.rem(at[1] + (4 - k), 4)
        blocks = []
        for pair in range(2):
            head = 4 * group + 2 * pair + column // VALUE_SIZE
            spread = jnp.where((slot < 48) & (slot % 16 == head), 1.0, 0.0).astype(BF)
            wide = jnp.dot(levels, spread, preferred_element_type=F32)
            level = [wide[i * rows : (i + 1) * rows] for i in range(4)]
            top = jnp.maximum(jnp.maximum(level[0], level[1]), jnp.maximum(level[2], level[3]))
            above = jnp.zeros((rows, LANES), F32)
            below = jnp.zeros((rows, LANES), F32)
            for one, part in zip(level, parts):
                share = jnp.exp2(one - top)
                above += share * part[2 * group + pair].astype(F32)
                below += share
            blocks.append((above / below).astype(BF))
        total += jnp.dot(
            jnp.concatenate(blocks, axis=1), weight[...], preferred_element_type=F32
        )
    mixed[...] = total
    norm = lax.rsqrt(jnp.mean(total * total, axis=-1, keepdims=True) + 1e-06)
    normed = (total * norm * gain[...]).astype(BF)
    half = normed_a.shape[1]
    normed_a[...] = normed[:, :half]
    normed_b[...] = normed[:, half:]


def feed_body(*refs):
    pieces, weights, refs = refs[:8], refs[8], refs[9:]
    ends, (rows_in, kept, gate, up, hidden, sems) = refs[:8], refs[8:]
    phases, per, _, share, width = kept.shape
    own, half = pieces[0].shape
    cut = rows_in.shape[2]

    def copy_of(chunk, member, first, count, sem):
        spot = (chunk, member, pl.ds(first, count))
        return pltpu.make_async_copy(weights.at[spot], kept.at[spot], sem)

    def early(chunk, member):
        return copy_of(chunk, member, 0, 2, sems.at[0, chunk, member])

    def late(chunk, member):
        return copy_of(chunk, member, 2, 1, sems.at[1, chunk, member])

    for make in (early, late):
        for chunk in range(phases):
            for member in range(per):
                make(chunk, member).start()
    for chunk in range(phases):
        side, at = divmod(chunk * cut, half)
        for k in range(4):
            rows_in[chunk, k * own : (k + 1) * own] = pieces[2 * k + side][:, at : at + cut]
    gate[...] = jnp.zeros(gate.shape, F32)
    up[...] = jnp.zeros(up.shape, F32)

    def widen(chunk, carry):
        for member in range(per):
            early(chunk, member).wait()
        rows = rows_in[chunk]
        gate[...] += jnp.dot(
            rows, kept[chunk, :, 0].reshape(per * share, width), preferred_element_type=F32
        )
        up[...] += jnp.dot(
            rows, kept[chunk, :, 1].reshape(per * share, width), preferred_element_type=F32
        )
        return carry

    lax.fori_loop(0, phases, widen, 0)
    value = gate[...]
    hidden[...] = (value / (1.0 + jnp.exp(-value)) * up[...]).astype(BF)
    for chunk in range(phases):
        for member in range(per):
            late(chunk, member).wait()
        terms = lax.dot_general(
            hidden[...],
            kept[chunk, :, 2].reshape(per * share, width),
            NT,
            preferred_element_type=F32,
        ).astype(BF)
        side, at = divmod(chunk * cut, half)
        for k in range(4):
            ends[4 * side + k][:, at : at + cut] = terms[k * own : (k + 1) * own]


def room(mib):
    return pltpu.CompilerParams(vmem_limit_bytes=mib * 1024 * 1024)


def whole(shape):
    return pl.BlockSpec(shape, lambda *_: (0,) * len(shape))


def layer(
    query_nope,
    query_rope,
    token_latent,
    key_rope,
    latent_norm_gain,
    key_expand_weight,
    value_expand_weight,
    residual,
    out_weight,
    ffn_gain,
    gate_weight,
    up_weight,
    down_weight,
):
    rows = query_nope.shape[0]
    members = lax.axis_size("tp")
    own = rows // members
    sp_count = lax.axis_size("z") * CORES
    tp_index = lax.axis_index("tp")
    sp_index = lax.axis_index("z") * CORES + lax.axis_index("core")
    at = jnp.stack([sp_index, tp_index]).astype(jnp.int32)
    rank = token_latent.shape[1]
    nope_width = query_nope.shape[1]
    rope_width = query_rope.shape[1]
    model = residual.shape[1]
    hidden_here = gate_weight.shape[1]
    share = gate_weight.shape[0]

    shards = jnp.concatenate([gate_weight, up_weight, down_weight.T], axis=0)
    gathered = lax.all_gather(shards, ("z", "core"), axis=0, tiled=True)

    freqs = ROPE // 4
    inverse = np.power(10000.0, -np.arange(freqs, dtype=np.float32) / freqs).astype(np.float32)
    inverse = jnp.asarray(np.tile(inverse, LANES // freqs)[None])
    packed, query = pl.pallas_call(
        prepare_body,
        grid_spec=pltpu.PrefetchScalarGridSpec(
            num_scalar_prefetch=1,
            grid=(1,),
            in_specs=[
                whole((1, LANES)),
                pl.BlockSpec((own, rank), lambda s, a: (a[1], 0)),
                whole((1, rank)),
                pl.BlockSpec((own, ROPE), lambda s, a: (a[1], 0)),
                whole((rows, nope_width)),
                whole((rows, rope_width)),
            ],
            out_specs=[whole((own, rank + LANES)), whole((rows, nope_width + rope_width))],
            scratch_shapes=[pltpu.VMEM((rows, LANES), F32), pltpu.VMEM((rows, LANES), F32)],
        ),
        out_shape=[
            jax.ShapeDtypeStruct((own, rank + LANES), BF),
            jax.ShapeDtypeStruct((rows, nope_width + rope_width), BF),
        ],
        compiler_params=room(8),
        name="prepare",
    )(at, inverse, token_latent, latent_norm_gain[None], key_rope, query_nope, query_rope)

    others = [shifted(query, "tp", k) for k in range(1, members)]
    near = lax.all_gather(packed, "z", axis=0, tiled=True)
    far = shifted(near, "core", 1)
    outs = [out_weight] + [shifted(out_weight, "tp", k) for k in range(1, members)]

    keys_here = 2 * near.shape[0]
    blocks = members * nope_width // LANES
    part = (blocks + 1, own, LANES)

    def group_at(s, a):
        return lax.rem(a[1] + members - s // 2, members)

    attended = pl.pallas_call(
        attend_body,
        grid_spec=pltpu.PrefetchScalarGridSpec(
            num_scalar_prefetch=1,
            grid=(blocks,),
            in_specs=[whole(query.shape)] * members
            + [whole(near.shape)] * 2
            + [pl.BlockSpec((rank, LANES), lambda s, a: (0, 2 * group_at(s, a) + s % 2))] * 2,
            out_specs=[whole(part)] * members,
            scratch_shapes=[
                pltpu.VMEM((blocks + 1, rows, LANES), BF),
                pltpu.VMEM((2 * rows, 2 * LANES), BF),
                pltpu.VMEM((keys_here, 2 * LANES), BF),
                pltpu.VMEM((2 * rows, keys_here), F32),
                pltpu.VMEM((2 * rows, LANES), F32),
                pltpu.VMEM((rows, LANES), F32),
            ],
        ),
        out_shape=[jax.ShapeDtypeStruct(part, BF)] * members,
        compiler_params=room(32),
        name="attend",
    )(at, query, *others, near, far, key_expand_weight, value_expand_weight)
    parts = [attended[0]] + [shifted(attended[k], "tp", k) for k in range(1, members)]
    half = model // 2
    mixed, own_a, own_b = pl.pallas_call(
        merge_body,
        grid_spec=pltpu.PrefetchScalarGridSpec(
            num_scalar_prefetch=1,
            grid=(1,),
            in_specs=[whole(part)] * members
            + [whole(out_weight.shape)] * members
            + [pl.BlockSpec((own, model), lambda s, a: (a[1], 0)), whole((1, model))],
            out_specs=[whole((own, model)), whole((own, half)), whole((own, half))],
        ),
        out_shape=[
            jax.ShapeDtypeStruct((own, model), F32),
            jax.ShapeDtypeStruct((own, half), BF),
            jax.ShapeDtypeStruct((own, half), BF),
        ],
        compiler_params=room(20),
        name="merge",
    )(at, *parts, *outs, residual, ffn_gain[None])
    below_a = shifted(own_a, "tp", 1)
    above_b = shifted(own_b, "tp", -1)
    below_b = shifted(own_b, "tp", 1)
    above_a = shifted(own_a, "tp", -1)
    across_a = shifted(below_a, "tp", 1)
    across_b = shifted(above_b, "tp", -1)

    phases = 4
    cut = model // phases
    weights = gathered.reshape(phases, sp_count // phases, 3, share, hidden_here)
    terms = pl.pallas_call(
        feed_body,
        in_specs=[pl.BlockSpec(memory_space=pltpu.VMEM)] * 8 + [pl.BlockSpec(memory_space=pl.ANY)],
        out_specs=[pl.BlockSpec(memory_space=pltpu.VMEM)] * 8,
        out_shape=[jax.ShapeDtypeStruct((own, half), BF)] * 8,
        scratch_shapes=[
            pltpu.VMEM((phases, rows, cut), BF),
            pltpu.VMEM(weights.shape, BF),
            pltpu.VMEM((rows, hidden_here), F32),
            pltpu.VMEM((rows, hidden_here), F32),
            pltpu.VMEM((rows, hidden_here), BF),
            pltpu.SemaphoreType.DMA((2, phases, sp_count // phases)),
        ],
        compiler_params=room(40),
        name="feed",
    )(own_a, own_b, below_a, below_b, across_a, across_b, above_a, above_b, weights)
    mine_a, down_a, far_a, up_a, mine_b, down_b, far_b, up_b = terms
    far_a = shifted(far_a, "tp", -1)
    far_b = shifted(far_b, "tp", 1)
    from_above_b = shifted(down_b, "tp", -1)
    from_below_a = shifted(up_a, "tp", 1)
    from_above_a = shifted((down_a.astype(F32) + far_a.astype(F32)).astype(BF), "tp", -1)
    from_below_b = shifted((up_b.astype(F32) + far_b.astype(F32)).astype(BF), "tp", 1)

    def added(base, *more):
        for one in more:
            base = base + one.astype(F32)
        return base.astype(BF)

    return jnp.concatenate(
        [
            added(mixed[:, :half], mine_a, from_above_a, from_below_a),
            added(mixed[:, half:], mine_b, from_above_b, from_below_b),
        ],
        axis=1,
    )


def solution(mesh):
    groups, sp_count, members = mesh.devices.shape
    finer = Mesh(
        mesh.devices.reshape(groups, sp_count // CORES, CORES, members),
        ("grp", "z", "core", "tp"),
    )
    tokens = ("grp", "z", "core")
    return jax.shard_map(
        layer,
        mesh=finer,
        in_specs=(
            P(tokens, "tp"),
            P(tokens, "tp"),
            P(tokens, None),
            P(tokens, None),
            P(),
            P(),
            P(),
            P(tokens, None),
            P("tp", None),
            P(),
            P(("z", "core"), "tp"),
            P(("z", "core"), "tp"),
            P("tp", ("z", "core")),
        ),
        out_specs=P(tokens + ("tp",), None),
        check_vma=False,
    )
```

time: 270 us -> 234 us (0.87)
  the two profiles are of different devices: /device:TPU:33 before, /device:TPU:40 now
where the time goes in v2:
time: 234 us
  blocking collectives  67.3 us (29%)
  waiting for transfers between devices  55.4 us (24%)
  starting transfers between devices  49.9 us (21%)
  Pallas kernels  41.4 us (18%)
  between operations  13.5 us (6%)
  other arithmetic  3.15 us (1%)
  local copies, waits for them, and re-layouts  3.1 us (1%)
    all_gather x1, blocking collectives, layer(): near = lax.all_gather(packed, 'z', axis=0, tiled=True)  67.3 us
    ppermute x22, waiting for transfers between devices, shifted(): lax.ppermute(array, axis, [(i, (i + step) % count) for i in range(count)])  55.4 us
    ppermute x22, starting transfers between devices, shifted(): lax.ppermute(array, axis, [(i, (i + step) % count) for i in range(count)])  49.9 us
    pallas_call x1, Pallas kernels, layer(): pl.pallas_call(attend_body, grid_spec=pltpu.PrefetchScalarGridSpec(num_sc...  27.3 us
    pallas_call x1, Pallas kernels, layer(): pl.pallas_call(feed_body, in_specs=[pl.BlockSpec(memory_space=pltpu.VMEM)...  10.5 us
  transfers between devices with their start and end apart: 23, of which 11 were waited for; matrix products, arithmetic and copies ran while one was open for 0% of the time, Pallas kernels for 13%

profile of v2, /device:TPU:40, one launch (start us, length us, event | category | flops | bytes accessed | tf_op | source)
XLA Modules:
  0.0 233.7 jit_solution(7003824752342818475)
XLA Ops:
  6.6 2.1 pad_maximum_fusion
  8.7 1.7 collective-permute-start.7
  10.4 0.9 copy.15.key
  11.4 0.9 copy-done.6
  13.6 1.3 prepare.1
  14.9 67.3 %all_gather.6.near = bf16[1280,384]{1,0:T(8,128)(2,1)S(1)} all-gather(bf16[80,384]{1,0:T(8,128)(2,1)S(1)} %get-tuple-element.23), channel_id=1, replica_groups=mesh['grp'=2,'z'=16,'core'=2,'tp'=4] {'z'}, dimensions={0}, use_global_device_ids=true | all-gather | bytes 1044480 | tf_op jit(solution)/shard_map/all_gather | solution.py:308
  82.1 3.0 %collective-permute-start.8 = (bf16[256,2048]{1,0:T(8,128)(2,1)S(1)}, bf16[256,2048]{1,0:T(8,128)(2,1)S(1)}, u32[]{:S(2)}, u32[]{:S(2)}) collective-permute-start(bf16[256,2048]{1,0:T(8,128)(2,1)S(1)} %copy-done.1), channel_id=1, source_target_pairs={{0,2},{1,3},{2,0},{3,1},{4,6},{5,7},{6,4},{7,5},{8,10},{9,11},{10,... | collective-permute-start | bytes 3145736 | tf_op jit(solution)/shard_map/ppermute | solution.py:27
  85.1 1.3 collective-permute-start.9
  87.2 27.3 %collective-permute-done.q1 = bf16[320,384]{1,0:T(8,128)(2,1)S(1)} collective-permute-done((bf16[320,384]{1,0:T(8,128)(2,1)S(1)}, bf16[320,384]{1,0:T(8,128)(2,1)S(1)}, u32[]{:S(2)}, u32[]{:S(2)}) %collective-permute-start) | collective-permute-done | bytes 245792 | tf_op jit(solution)/shard_map/ppermute | solution.py:27
  114.5 3.0 %collective-permute-start.1 = (bf16[320,384]{1,0:T(8,128)(2,1)S(1)}, bf16[320,384]{1,0:T(8,128)(2,1)S(1)}, u32[]{:S(2)}, u32[]{:S(2)}) collective-permute-start(bf16[320,384]{1,0:T(8,128)(2,1)S(1)} %get-tuple-element.22.q0), channel_id=1, source_target_pairs={{0,2},{1,3},{2,0},{3,1},{4,6},{5,7},{6,4},{7,5},{8,10},{9,11},{10,... | collective-permute-start | bytes 737288 | tf_op jit(solution)/shard_map/ppermute | solution.py:27
  117.5 6.5 %collective-permute-done.1.q2 = bf16[320,384]{1,0:T(8,128)(2,1)S(1)} collective-permute-done((bf16[320,384]{1,0:T(8,128)(2,1)S(1)}, bf16[320,384]{1,0:T(8,128)(2,1)S(1)}, u32[]{:S(2)}, u32[]{:S(2)}) %collective-permute-start.1) | collective-permute-done | bytes 245792 | tf_op jit(solution)/shard_map/ppermute | solution.py:27
  124.0 14.8 %collective-permute-start.2 = (bf16[320,384]{1,0:T(8,128)(2,1)S(1)}, bf16[320,384]{1,0:T(8,128)(2,1)S(1)}, u32[]{:S(2)}, u32[]{:S(2)}) collective-permute-start(bf16[320,384]{1,0:T(8,128)(2,1)S(1)} %get-tuple-element.22.q0), channel_id=1, source_target_pairs={{0,3},{1,0},{2,1},{3,2},{4,7},{5,4},{6,5},{7,6},{8,11},{9,8},{10,9... | collective-permute-start | bytes 737288 | tf_op jit(solution)/shard_map/ppermute | solution.py:27
  138.8 5.7 %collective-permute-done.2.q3 = bf16[320,384]{1,0:T(8,128)(2,1)S(1)} collective-permute-done((bf16[320,384]{1,0:T(8,128)(2,1)S(1)}, bf16[320,384]{1,0:T(8,128)(2,1)S(1)}, u32[]{:S(2)}, u32[]{:S(2)}) %collective-permute-start.2) | collective-permute-done | bytes 245792 | tf_op jit(solution)/shard_map/ppermute | solution.py:27
  144.5 27.3 %attend.1 = (bf16[9,80,128]{2,1,0:T(8,128)(2,1)S(1)}, bf16[9,80,128]{2,1,0:T(8,128)(2,1)S(1)}, bf16[9,80,128]{2,1,0:T(8,128)(2,1)S(1)}, bf16[9,80,128]{2,1,0:T(8,128)(2,1)S(1)}) custom-call(s32[2]{0:T(128)S(1)} %pad_add_fusion.at, bf16[320,384]{1,0:T(8,128)(2,1)S(1)} %get-tuple-element.22.q0, bf16[320,384]{1,0:T(8,128)(2,1)S(1)} %collective-permute-done.q1, ...), custom_call_target="tpu_custom_call" | custom-call | tf_op jit(solution)/shard_map/attend/pallas_call | solution.py:319
  171.9 1.9 collective-permute-start.4
  173.7 2.7 %collective-permute-start.5 = (bf16[9,80,128]{2,1,0:T(8,128)(2,1)S(1)}, bf16[9,80,128]{2,1,0:T(8,128)(2,1)S(1)}, u32[]{:S(2)}, u32[]{:S(2)}) collective-permute-start(bf16[9,80,128]{2,1,0:T(8,128)(2,1)S(1)} %get-tuple-element.26), channel_id=1, source_target_pairs={{0,2},{1,3},{2,0},{3,1},{4,6},{5,7},{6,4},{7,5},{8,10},{9,11},{10,... | collective-permute-start | bytes 552968 | tf_op jit(solution)/shard_map/ppermute | solution.py:27
  176.6 3.8 %collective-permute-done.4.p1 = bf16[9,80,128]{2,1,0:T(8,128)(2,1)S(1)} collective-permute-done((bf16[9,80,128]{2,1,0:T(8,128)(2,1)S(1)}, bf16[9,80,128]{2,1,0:T(8,128)(2,1)S(1)}, u32[]{:S(2)}, u32[]{:S(2)}) %collective-permute-start.4) | collective-permute-done | bytes 184352 | tf_op jit(solution)/shard_map/ppermute | solution.py:27
  180.4 3.3 %collective-permute-done.5.p2 = bf16[9,80,128]{2,1,0:T(8,128)(2,1)S(1)} collective-permute-done((bf16[9,80,128]{2,1,0:T(8,128)(2,1)S(1)}, bf16[9,80,128]{2,1,0:T(8,128)(2,1)S(1)}, u32[]{:S(2)}, u32[]{:S(2)}) %collective-permute-start.5) | collective-permute-done | bytes 184352 | tf_op jit(solution)/shard_map/ppermute | solution.py:27
  183.7 2.3 %merge.1 = (f32[80,2048]{1,0:T(8,128)S(1)}, bf16[80,1024]{1,0:T(8,128)(2,1)S(1)}, bf16[80,1024]{1,0:T(8,128)(2,1)S(1)}) custom-call(s32[2]{0:T(128)S(1)} %pad_add_fusion.at, bf16[9,80,128]{2,1,0:T(8,128)(2,1)S(1)} %get-tuple-element.24.p0, bf16[9,80,128]{2,1,0:T(8,128)(2,1)S(1)} %collective-permute-done.4.p1, ...), custom_call_target="tpu_custom_call" | custom-call | tf_op jit(solution)/shard_map/merge/pallas_call | solution.py:343
  186.0 1.2 collective-permute-start.10
  187.2 2.1 collective-permute-start.13
  189.4 3.2 %collective-permute-start.15 = (bf16[80,1024]{1,0:T(8,128)(2,1)S(1)}, bf16[80,1024]{1,0:T(8,128)(2,1)S(1)}, u32[]{:S(2)}, u32[]{:S(2)}) collective-permute-start(bf16[80,1024]{1,0:T(8,128)(2,1)S(1)} %get-tuple-element.29.refs_0_), channel_id=1, source_target_pairs={{0,3},{1,0},{2,1},{3,2},{4,7},{5,4},{6,5},{7,6},{8,11},{9,8},{10,9... | collective-permute-start | bytes 491528 | tf_op jit(solution)/shard_map/ppermute | solution.py:27
  192.6 0.9 collective-permute-done.10.refs_2_
  193.5 0.8 collective-permute-start.12
  194.3 2.7 %collective-permute-start.14 = (bf16[80,1024]{1,0:T(8,128)(2,1)S(1)}, bf16[80,1024]{1,0:T(8,128)(2,1)S(1)}, u32[]{:S(2)}, u32[]{:S(2)}) collective-permute-start(bf16[80,1024]{1,0:T(8,128)(2,1)S(1)} %collective-permute-done.13.refs_7_), channel_id=1, source_target_pairs={{0,3},{1,0},{2,1},{3,2},{4,7},{5,4},{6,5},{7,6},{8,11},{9,8},{10,9... | collective-permute-start | bytes 491528 | tf_op jit(solution)/shard_map/ppermute | solution.py:27
  197.8 2.3 collective-permute-done.12.refs_4_
  200.1 10.5 %feed.1 = (bf16[80,1024]{1,0:T(8,128)(2,1)S(1)}, bf16[80,1024]{1,0:T(8,128)(2,1)S(1)}, bf16[80,1024]{1,0:T(8,128)(2,1)S(1)}, bf16[80,1024]{1,0:T(8,128)(2,1)S(1)...) custom-call(bf16[80,1024]{1,0:T(8,128)(2,1)S(1)} %get-tuple-element., ...), custom_call_target="tpu_custom_call" | custom-call | tf_op jit(solution)/shard_map/feed/pallas_call | solution.py:371
  211.2 3.1 %collective-permute-start.16 = (bf16[80,1024]{1,0:T(8,128)(2,1)S(1)}, bf16[80,1024]{1,0:T(8,128)(2,1)S(1)}, u32[]{:S(2)}, u32[]{:S(2)}) collective-permute-start(bf16[80,1024]{1,0:T(8,128)(2,1)S(1)} %get-tuple-element.33), channel_id=1, source_target_pairs={{0,3},{1,0},{2,1},{3,2},{4,7},{5,4},{6,5},{7,6},{8,11},{9,8},{10,9... | collective-permute-start | bytes 491528 | tf_op jit(solution)/shard_map/ppermute | solution.py:27
  214.3 3.2 %collective-permute-start.19 = (bf16[80,1024]{1,0:T(8,128)(2,1)S(1)}, bf16[80,1024]{1,0:T(8,128)(2,1)S(1)}, u32[]{:S(2)}, u32[]{:S(2)}) collective-permute-start(bf16[80,1024]{1,0:T(8,128)(2,1)S(1)} %get-tuple-element.36), channel_id=1, source_target_pairs={{0,3},{1,0},{2,1},{3,2},{4,7},{5,4},{6,5},{7,6},{8,11},{9,8},{10,9... | collective-permute-start | bytes 491528 | tf_op jit(solution)/shard_map/ppermute | solution.py:27
  217.5 1.7 collective-permute-done.20
  219.5 3.3 %collective-permute-start.17 = (bf16[80,1024]{1,0:T(8,128)(2,1)S(1)}, bf16[80,1024]{1,0:T(8,128)(2,1)S(1)}, u32[]{:S(2)}, u32[]{:S(2)}) collective-permute-start(bf16[80,1024]{1,0:T(8,128)(2,1)S(1)} %add_convert_fusion.3), channel_id=1, source_target_pairs={{0,3},{1,0},{2,1},{3,2},{4,7},{5,4},{6,5},{7,6},{8,11},{9,8},{10,9... | collective-permute-start | bytes 491528 | tf_op jit(solution)/shard_map/ppermute | solution.py:27
  222.8 3.1 %collective-permute-done.21 = bf16[80,1024]{1,0:T(8,128)(2,1)S(1)} collective-permute-done((bf16[80,1024]{1,0:T(8,128)(2,1)S(1)}, bf16[80,1024]{1,0:T(8,128)(2,1)S(1)}, u32[]{:S(2)}, u32[]{:S(2)}) %collective-permute-start.21) | collective-permute-done | bytes 163872 | tf_op jit(solution)/shard_map/ppermute | solution.py:27
  (47 shorter events, 4.9 us)
Async XLA Ops:
  6.5 2.1 copy-start.1
  6.5 4.8 %copy-start.5 = (bf16[320,256]{1,0:T(8,128)(2,1)S(1)}, bf16[320,256]{1,0:T(8,128)(2,1)}, u32[]{:S(2)}) copy-start(bf16[320,256]{1,0:T(8,128)(2,1)} %nope.1) | copy-start | bytes 491524
  6.6 4.8 %copy-start.4 = (bf16[320,256]{1,0:T(8,128)(2,1)S(1)}, bf16[320,256]{1,0:T(8,128)(2,1)}, u32[]{:S(2)}) copy-start(bf16[320,256]{1,0:T(8,128)(2,1)} %lat.1) | copy-start | bytes 491524
  6.6 193.5 %all-gather.2.cloned.1.call-start = ((), (), s32[]{:S(2)}) async-start(), calls=%async_computation | async-start | bytes 17842176 | tf_op jit(solution)/shard_map/all_gather | solution.py:278
  8.6 135.9 %copy-start.2 = (bf16[256,1024]{1,0:T(8,128)(2,1)S(1)}, bf16[256,1024]{1,0:T(8,128)(2,1)}, u32[]{:S(2)}) copy-start(bf16[256,1024]{1,0:T(8,128)(2,1)} %key_w.1) | copy-start | bytes 1572868
  8.6 135.9 %copy-start.3 = (bf16[256,1024]{1,0:T(8,128)(2,1)S(1)}, bf16[256,1024]{1,0:T(8,128)(2,1)}, u32[]{:S(2)}) copy-start(bf16[256,1024]{1,0:T(8,128)(2,1)} %value_w.1) | copy-start | bytes 1572868
  8.7 167.8 %collective-permute-start.7 = (bf16[256,2048]{1,0:T(8,128)(2,1)S(1)}, bf16[256,2048]{1,0:T(8,128)(2,1)S(1)}, u32[]{:S(2)}, u32[]{:S(2)}) collective-permute-start(bf16[256,2048]{1,0:T(8,128)(2,1)S(1)} %copy-done.1), channel_id=1, source_target_pairs={{0,1},{1,2},{2,3},{3,0},{4,5},{5,6},{6,7},{7,4},{8,9},{9,10},{10,1... | collective-permute-start | bytes 3145736 | tf_op jit(solution)/shard_map/ppermute | solution.py:27
  11.4 0.9 copy-start.6
  12.3 0.7 copy-start.8
  82.1 62.4 %collective-permute-start.3 = (bf16[1280,384]{1,0:T(8,128)(2,1)S(1)}, bf16[1280,384]{1,0:T(8,128)(2,1)S(1)}, u32[]{:S(2)}, u32[]{:S(2)}) collective-permute-start(bf16[1280,384]{1,0:T(8,128)(2,1)S(1)} %all_gather.6.near), channel_id=1, source_target_pairs={{0,4},{4,0},{1,5},{5,1},{2,6},{6,2},{3,7},{7,3},{8,12},{12,8},{9,1... | collective-permute-start | bytes 2949128 | tf_op jit(solution)/shard_map/ppermute | solution.py:27
  82.1 94.4 %collective-permute-start.8 = (bf16[256,2048]{1,0:T(8,128)(2,1)S(1)}, bf16[256,2048]{1,0:T(8,128)(2,1)S(1)}, u32[]{:S(2)}, u32[]{:S(2)}) collective-permute-start(bf16[256,2048]{1,0:T(8,128)(2,1)S(1)} %copy-done.1), channel_id=1, source_target_pairs={{0,2},{1,3},{2,0},{3,1},{4,6},{5,7},{6,4},{7,5},{8,10},{9,11},{10,... | collective-permute-start | bytes 3145736 | tf_op jit(solution)/shard_map/ppermute | solution.py:27
  85.1 91.4 %collective-permute-start.9 = (bf16[256,2048]{1,0:T(8,128)(2,1)S(1)}, bf16[256,2048]{1,0:T(8,128)(2,1)S(1)}, u32[]{:S(2)}, u32[]{:S(2)}) collective-permute-start(bf16[256,2048]{1,0:T(8,128)(2,1)S(1)} %copy-done.1), channel_id=1, source_target_pairs={{0,3},{1,0},{2,1},{3,2},{4,7},{5,4},{6,5},{7,6},{8,11},{9,8},{10,9... | collective-permute-start | bytes 3145736 | tf_op jit(solution)/shard_map/ppermute | solution.py:27
  86.4 97.2 %copy-start = (bf16[320,2048]{1,0:T(8,128)(2,1)S(1)}, bf16[320,2048]{1,0:T(8,128)(2,1)}, u32[]{:S(2)}) copy-start(bf16[320,2048]{1,0:T(8,128)(2,1)} %residual.1) | copy-start | bytes 3932164
  86.4 97.2 %copy-start.7 = (f32[2048]{0:T(1024)S(1)}, f32[2048]{0:T(1024)}, u32[]{:S(2)}) copy-start(f32[2048]{0:T(1024)} %param.23) | copy-start | bytes 24580
  86.4 28.0 %collective-permute-start = (bf16[320,384]{1,0:T(8,128)(2,1)S(1)}, bf16[320,384]{1,0:T(8,128)(2,1)S(1)}, u32[]{:S(2)}, u32[]{:S(2)}) collective-permute-start(bf16[320,384]{1,0:T(8,128)(2,1)S(1)} %get-tuple-element.22.q0), channel_id=1, source_target_pairs={{0,1},{1,2},{2,3},{3,0},{4,5},{5,6},{6,7},{7,4},{8,9},{9,10},{10,1... | collective-permute-start | bytes 737288 | tf_op jit(solution)/shard_map/ppermute | solution.py:27
  114.5 9.5 %collective-permute-start.1 = (bf16[320,384]{1,0:T(8,128)(2,1)S(1)}, bf16[320,384]{1,0:T(8,128)(2,1)S(1)}, u32[]{:S(2)}, u32[]{:S(2)}) collective-permute-start(bf16[320,384]{1,0:T(8,128)(2,1)S(1)} %get-tuple-element.22.q0), channel_id=1, source_target_pairs={{0,2},{1,3},{2,0},{3,1},{4,6},{5,7},{6,4},{7,5},{8,10},{9,11},{10,... | collective-permute-start | bytes 737288 | tf_op jit(solution)/shard_map/ppermute | solution.py:27
  124.0 20.5 %collective-permute-start.2 = (bf16[320,384]{1,0:T(8,128)(2,1)S(1)}, bf16[320,384]{1,0:T(8,128)(2,1)S(1)}, u32[]{:S(2)}, u32[]{:S(2)}) collective-permute-start(bf16[320,384]{1,0:T(8,128)(2,1)S(1)} %get-tuple-element.22.q0), channel_id=1, source_target_pairs={{0,3},{1,0},{2,1},{3,2},{4,7},{5,4},{6,5},{7,6},{8,11},{9,8},{10,9... | collective-permute-start | bytes 737288 | tf_op jit(solution)/shard_map/ppermute | solution.py:27
  171.9 8.5 %collective-permute-start.4 = (bf16[9,80,128]{2,1,0:T(8,128)(2,1)S(1)}, bf16[9,80,128]{2,1,0:T(8,128)(2,1)S(1)}, u32[]{:S(2)}, u32[]{:S(2)}) collective-permute-start(bf16[9,80,128]{2,1,0:T(8,128)(2,1)S(1)} %get-tuple-element.25), channel_id=1, source_target_pairs={{0,1},{1,2},{2,3},{3,0},{4,5},{5,6},{6,7},{7,4},{8,9},{9,10},{10,1... | collective-permute-start | bytes 552968 | tf_op jit(solution)/shard_map/ppermute | solution.py:27
  173.7 9.9 %collective-permute-start.5 = (bf16[9,80,128]{2,1,0:T(8,128)(2,1)S(1)}, bf16[9,80,128]{2,1,0:T(8,128)(2,1)S(1)}, u32[]{:S(2)}, u32[]{:S(2)}) collective-permute-start(bf16[9,80,128]{2,1,0:T(8,128)(2,1)S(1)} %get-tuple-element.26), channel_id=1, source_target_pairs={{0,2},{1,3},{2,0},{3,1},{4,6},{5,7},{6,4},{7,5},{8,10},{9,11},{10,... | collective-permute-start | bytes 552968 | tf_op jit(solution)/shard_map/ppermute | solution.py:27
  176.5 7.2 %collective-permute-start.6 = (bf16[9,80,128]{2,1,0:T(8,128)(2,1)S(1)}, bf16[9,80,128]{2,1,0:T(8,128)(2,1)S(1)}, u32[]{:S(2)}, u32[]{:S(2)}) collective-permute-start(bf16[9,80,128]{2,1,0:T(8,128)(2,1)S(1)} %get-tuple-element.27), channel_id=1, source_target_pairs={{0,3},{1,0},{2,1},{3,2},{4,7},{5,4},{6,5},{7,6},{8,11},{9,8},{10,9... | collective-permute-start | bytes 552968 | tf_op jit(solution)/shard_map/ppermute | solution.py:27
  186.0 7.5 %collective-permute-start.10 = (bf16[80,1024]{1,0:T(8,128)(2,1)S(1)}, bf16[80,1024]{1,0:T(8,128)(2,1)S(1)}, u32[]{:S(2)}, u32[]{:S(2)}) collective-permute-start(bf16[80,1024]{1,0:T(8,128)(2,1)S(1)} %get-tuple-element.29.refs_0_), channel_id=1, source_target_pairs={{0,1},{1,2},{2,3},{3,0},{4,5},{5,6},{6,7},{7,4},{8,9},{9,10},{10,1... | collective-permute-start | bytes 491528 | tf_op jit(solution)/shard_map/ppermute | solution.py:27
  187.2 7.1 %collective-permute-start.13 = (bf16[80,1024]{1,0:T(8,128)(2,1)S(1)}, bf16[80,1024]{1,0:T(8,128)(2,1)S(1)}, u32[]{:S(2)}, u32[]{:S(2)}) collective-permute-start(bf16[80,1024]{1,0:T(8,128)(2,1)S(1)} %get-tuple-element.30.refs_1_), channel_id=1, source_target_pairs={{0,3},{1,0},{2,1},{3,2},{4,7},{5,4},{6,5},{7,6},{8,11},{9,8},{10,9... | collective-permute-start | bytes 491528 | tf_op jit(solution)/shard_map/ppermute | solution.py:27
  189.4 8.3 %collective-permute-start.11 = (bf16[80,1024]{1,0:T(8,128)(2,1)S(1)}, bf16[80,1024]{1,0:T(8,128)(2,1)S(1)}, u32[]{:S(2)}, u32[]{:S(2)}) collective-permute-start(bf16[80,1024]{1,0:T(8,128)(2,1)S(1)} %get-tuple-element.30.refs_1_), channel_id=1, source_target_pairs={{0,1},{1,2},{2,3},{3,0},{4,5},{5,6},{6,7},{7,4},{8,9},{9,10},{10,1... | collective-permute-start | bytes 491528 | tf_op jit(solution)/shard_map/ppermute | solution.py:27
  189.4 8.5 %collective-permute-start.15 = (bf16[80,1024]{1,0:T(8,128)(2,1)S(1)}, bf16[80,1024]{1,0:T(8,128)(2,1)S(1)}, u32[]{:S(2)}, u32[]{:S(2)}) collective-permute-start(bf16[80,1024]{1,0:T(8,128)(2,1)S(1)} %get-tuple-element.29.refs_0_), channel_id=1, source_target_pairs={{0,3},{1,0},{2,1},{3,2},{4,7},{5,4},{6,5},{7,6},{8,11},{9,8},{10,9... | collective-permute-start | bytes 491528 | tf_op jit(solution)/shard_map/ppermute | solution.py:27
  193.5 6.5 %collective-permute-start.12 = (bf16[80,1024]{1,0:T(8,128)(2,1)S(1)}, bf16[80,1024]{1,0:T(8,128)(2,1)S(1)}, u32[]{:S(2)}, u32[]{:S(2)}) collective-permute-start(bf16[80,1024]{1,0:T(8,128)(2,1)S(1)} %collective-permute-done.10.refs_2_), channel_id=1, source_target_pairs={{0,1},{1,2},{2,3},{3,0},{4,5},{5,6},{6,7},{7,4},{8,9},{9,10},{10,1... | collective-permute-start | bytes 491528 | tf_op jit(solution)/shard_map/ppermute | solution.py:27
  194.3 5.8 %collective-permute-start.14 = (bf16[80,1024]{1,0:T(8,128)(2,1)S(1)}, bf16[80,1024]{1,0:T(8,128)(2,1)S(1)}, u32[]{:S(2)}, u32[]{:S(2)}) collective-permute-start(bf16[80,1024]{1,0:T(8,128)(2,1)S(1)} %collective-permute-done.13.refs_7_), channel_id=1, source_target_pairs={{0,3},{1,0},{2,1},{3,2},{4,7},{5,4},{6,5},{7,6},{8,11},{9,8},{10,9... | collective-permute-start | bytes 491528 | tf_op jit(solution)/shard_map/ppermute | solution.py:27
  210.5 8.7 %collective-permute-start.20 = (bf16[80,1024]{1,0:T(8,128)(2,1)S(1)}, bf16[80,1024]{1,0:T(8,128)(2,1)S(1)}, u32[]{:S(2)}, u32[]{:S(2)}) collective-permute-start(bf16[80,1024]{1,0:T(8,128)(2,1)S(1)} %get-tuple-element.38), channel_id=1, source_target_pairs={{0,1},{1,2},{2,3},{3,0},{4,5},{5,6},{6,7},{7,4},{8,9},{9,10},{10,1... | collective-permute-start | bytes 491528 | tf_op jit(solution)/shard_map/ppermute | solution.py:27
  211.2 8.2 %collective-permute-start.16 = (bf16[80,1024]{1,0:T(8,128)(2,1)S(1)}, bf16[80,1024]{1,0:T(8,128)(2,1)S(1)}, u32[]{:S(2)}, u32[]{:S(2)}) collective-permute-start(bf16[80,1024]{1,0:T(8,128)(2,1)S(1)} %get-tuple-element.33), channel_id=1, source_target_pairs={{0,3},{1,0},{2,1},{3,2},{4,7},{5,4},{6,5},{7,6},{8,11},{9,8},{10,9... | collective-permute-start | bytes 491528 | tf_op jit(solution)/shard_map/ppermute | solution.py:27
  214.3 8.5 %collective-permute-start.18 = (bf16[80,1024]{1,0:T(8,128)(2,1)S(1)}, bf16[80,1024]{1,0:T(8,128)(2,1)S(1)}, u32[]{:S(2)}, u32[]{:S(2)}) collective-permute-start(bf16[80,1024]{1,0:T(8,128)(2,1)S(1)} %get-tuple-element.34), channel_id=1, source_target_pairs={{0,1},{1,2},{2,3},{3,0},{4,5},{5,6},{6,7},{7,4},{8,9},{9,10},{10,1... | collective-permute-start | bytes 491528 | tf_op jit(solution)/shard_map/ppermute | solution.py:27
  214.3 8.5 %collective-permute-start.19 = (bf16[80,1024]{1,0:T(8,128)(2,1)S(1)}, bf16[80,1024]{1,0:T(8,128)(2,1)S(1)}, u32[]{:S(2)}, u32[]{:S(2)}) collective-permute-start(bf16[80,1024]{1,0:T(8,128)(2,1)S(1)} %get-tuple-element.36), channel_id=1, source_target_pairs={{0,3},{1,0},{2,1},{3,2},{4,7},{5,4},{6,5},{7,6},{8,11},{9,8},{10,9... | collective-permute-start | bytes 491528 | tf_op jit(solution)/shard_map/ppermute | solution.py:27
  219.3 6.6 %collective-permute-start.21 = (bf16[80,1024]{1,0:T(8,128)(2,1)S(1)}, bf16[80,1024]{1,0:T(8,128)(2,1)S(1)}, u32[]{:S(2)}, u32[]{:S(2)}) collective-permute-start(bf16[80,1024]{1,0:T(8,128)(2,1)S(1)} %add_convert_fusion.1), channel_id=1, source_target_pairs={{0,1},{1,2},{2,3},{3,0},{4,5},{5,6},{6,7},{7,4},{8,9},{9,10},{10,1... | collective-permute-start | bytes 491528 | tf_op jit(solution)/shard_map/ppermute | solution.py:27
  219.5 6.4 %collective-permute-start.17 = (bf16[80,1024]{1,0:T(8,128)(2,1)S(1)}, bf16[80,1024]{1,0:T(8,128)(2,1)S(1)}, u32[]{:S(2)}, u32[]{:S(2)}) collective-permute-start(bf16[80,1024]{1,0:T(8,128)(2,1)S(1)} %add_convert_fusion.3), channel_id=1, source_target_pairs={{0,3},{1,0},{2,1},{3,2},{4,7},{5,4},{6,5},{7,6},{8,11},{9,8},{10,9... | collective-permute-start | bytes 491528 | tf_op jit(solution)/shard_map/ppermute | solution.py:27
  (1 other events, 0.7 us)
Sparse Core Ops, SparseCore 0:
  9.2 129.9 all-gather.1

commit v3 on v2

--- a/solution.py
+++ b/solution.py
@@ -15,6 +15,7 @@
 GRID_W = 64
 LANES = 128
 CORES = 2
+PART = 16
 BF = jnp.bfloat16
 F32 = jnp.float32
 
@@ -31,12 +32,21 @@
     return lax.broadcasted_iota(jnp.int32, shape, len(shape) - 1)
 
 
+def close_body(mixed, a0, a1, a2, b0, b1, b2, out):
+    half = a0.shape[1]
+    for at, parts in ((0, (a0, a1, a2)), (half, (b0, b1, b2))):
+        total = mixed[:, at : at + half]
+        for part in parts:
+            total += part[...].astype(F32)
+        out[:, at : at + half] = total.astype(BF)
+
+
 def prepare_body(at, inverse, lat, gain, key, nope, rope, packed, query, cos_s, sin_s):
     rows = rope.shape[0]
-    own = packed.shape[0]
-    first = at[0] * rows
+    own = lat.shape[0]
+    start = at[0] * rows
     lane = lane_index((rows, LANES))
-    position = first + lax.broadcasted_iota(jnp.int32, (rows, LANES), 0)
+    position = start + lax.broadcasted_iota(jnp.int32, (rows, LANES), 0)
     place = jnp.where((lane & 16) == 0, position >> int(math.log2(GRID_W)), position & (GRID_W - 1))
     angle = place.astype(F32) * inverse[...]
     cos_s[...] = jnp.cos(angle)
@@ -55,13 +65,22 @@
     rank = lat.shape[1]
     wide = lat[...].astype(F32)
     scale = lax.rsqrt(jnp.mean(wide * wide, axis=-1, keepdims=True) + 1e-06)
-    packed[:, :rank] = (wide * scale * gain[...]).astype(BF)
+    normed = (wide * scale * gain[...]).astype(BF)
+    for j in range(rank // LANES):
+        packed[j * own : (j + 1) * own] = normed[:, j * LANES : (j + 1) * LANES]
     four = jnp.concatenate([key[...]] * (LANES // ROPE), axis=1)
-    packed[:, rank:] = turn(four, cos_s[mine, :], sin_s[mine, :])
+    turned = turn(four, cos_s[mine, :], sin_s[mine, :])
+    place = lane_index((PART, LANES)) // ROPE
+    first = turned[:PART]
+    for j in range(1, LANES // ROPE):
+        first = jnp.where(place == j, turned[j * PART : (j + 1) * PART], first)
+    at_row = rank // LANES * own
+    packed[at_row : at_row + PART] = first
+    packed[at_row + PART : at_row + 2 * PART] = turned[LANES // ROPE * PART :]
 
 
 def attend_body(
-    at, q0, q1, q2, q3, near, far, key_w, value_w, o0, o1, o2, o3, held, stacked, values, scores, highest, stats
+    at, q0, q1, q2, q3, near, far, key_w, value_w, o0, o1, o2, o3, held, stacked, latents, ropes, values, scores, highest, stats
 ):
     step = pl.program_id(0)
     last = pl.num_programs(0) - 1
@@ -70,7 +89,8 @@
     group = lax.rem(at[1] + 4 - turn, 4)
     rows = q0.shape[0]
     own = o0.shape[1]
-    half = near.shape[0]
+    places = near.shape[0]
+    half = places * own
     rank = key_w.shape[0]
     scale = (UNROTATED_SIZE + ROPE) ** (-0.5) * math.log2(math.e)
     tile = 256
@@ -82,6 +102,27 @@
     def _():
         values[:, LANES:] = jnp.ones((2 * half, LANES), BF)
         stats[...] = jnp.zeros(stats.shape, F32)
+        splits = LANES // ROPE
+        head_row = rank // LANES * own
+        spot = lane_index((places * PART, LANES)) // ROPE
+        for h, source in enumerate((near, far)):
+            mixed = source[:, head_row : head_row + PART].reshape(places * PART, LANES).astype(F32)
+            rolled = [mixed] + [pltpu.roll(mixed, ROPE * k, 1) for k in range(1, splits)]
+            for j in range(splits):
+                full = rolled[(splits - j) % splits]
+                for lanes_at in range(1, splits):
+                    full = jnp.where(spot == lanes_at, rolled[(lanes_at - j) % splits], full)
+                full = full.astype(BF)
+                for z in range(places):
+                    row = h * half + z * own + j * PART
+                    ropes[row : row + PART] = full[z * PART : (z + 1) * PART]
+            for z in range(places):
+                row = h * half + z * own
+                ropes[row + splits * PART : row + own] = source[z, head_row + PART :]
+                for j in range(rank // LANES):
+                    latents[row : row + own, j * LANES : (j + 1) * LANES] = source[
+                        z, j * own : (j + 1) * own
+                    ]
 
     zero = jnp.zeros((rows, LANES), BF)
     for k, query in enumerate((q0, q1, q2, q3)):
@@ -101,14 +142,12 @@
     for c in range(chunks):
         top = None
         for u in (c, c + chunks):
-            source, from_row = (near, u * tile) if u < chunks else (far, u * tile - half)
-            made = jnp.dot(
-                source[from_row : from_row + tile, :rank], both, preferred_element_type=F32
-            ).astype(BF)
-            values[u * tile : (u + 1) * tile, :LANES] = made[:, LANES:]
-            keys = jnp.concatenate([made[:, :LANES], source[from_row : from_row + tile, rank:]], axis=1)
+            spot = slice(u * tile, (u + 1) * tile)
+            made = jnp.dot(latents[spot], both, preferred_element_type=F32).astype(BF)
+            values[spot, :LANES] = made[:, LANES:]
+            keys = jnp.concatenate([made[:, :LANES], ropes[spot]], axis=1)
             part = lax.dot_general(asked, keys, NT, preferred_element_type=F32)
-            scores[:, u * tile : (u + 1) * tile] = part
+            scores[:, spot] = part
             level = jnp.maximum(part[:, :LANES], part[:, LANES:])
             top = level if top is None else jnp.maximum(top, level)
         highest[...] = top if c == 0 else jnp.maximum(highest[...], top)
@@ -197,10 +236,12 @@
     def late(chunk, member):
         return copy_of(chunk, member, 2, 1, sems.at[1, chunk, member])
 
-    for make in (early, late):
-        for chunk in range(phases):
-            for member in range(per):
-                make(chunk, member).start()
+    def begin(make, chunk):
+        for member in range(per):
+            make(chunk, member).start()
+
+    begin(early, 0)
+    begin(early, 1)
     for chunk in range(phases):
         side, at = divmod(chunk * cut, half)
         for k in range(4):
@@ -211,6 +252,15 @@
     def widen(chunk, carry):
         for member in range(per):
             early(chunk, member).wait()
+
+        @pl.when(chunk + 2 < phases)
+        def _():
+            begin(early, chunk + 2)
+
+        @pl.when(chunk + 2 >= phases)
+        def _():
+            begin(late, chunk + 2 - phases)
+
         rows = rows_in[chunk]
         gate[...] += jnp.dot(
             rows, kept[chunk, :, 0].reshape(per * share, width), preferred_element_type=F32
@@ -221,6 +271,8 @@
         return carry
 
     lax.fori_loop(0, phases, widen, 0)
+    for chunk in range(2, phases):
+        begin(late, chunk)
     value = gate[...]
     hidden[...] = (value / (1.0 + jnp.exp(-value)) * up[...]).astype(BF)
     for chunk in range(phases):
@@ -280,6 +332,7 @@
     freqs = ROPE // 4
     inverse = np.power(10000.0, -np.arange(freqs, dtype=np.float32) / freqs).astype(np.float32)
     inverse = jnp.asarray(np.tile(inverse, LANES // freqs)[None])
+    packed_shape = (rank // LANES * own + 2 * PART, LANES)
     packed, query = pl.pallas_call(
         prepare_body,
         grid_spec=pltpu.PrefetchScalarGridSpec(
@@ -293,11 +346,11 @@
                 whole((rows, nope_width)),
                 whole((rows, rope_width)),
             ],
-            out_specs=[whole((own, rank + LANES)), whole((rows, nope_width + rope_width))],
+            out_specs=[whole(packed_shape), whole((rows, nope_width + rope_width))],
             scratch_shapes=[pltpu.VMEM((rows, LANES), F32), pltpu.VMEM((rows, LANES), F32)],
         ),
         out_shape=[
-            jax.ShapeDtypeStruct((own, rank + LANES), BF),
+            jax.ShapeDtypeStruct(packed_shape, BF),
             jax.ShapeDtypeStruct((rows, nope_width + rope_width), BF),
         ],
         compiler_params=room(8),
@@ -306,10 +359,11 @@
 
     others = [shifted(query, "tp", k) for k in range(1, members)]
     near = lax.all_gather(packed, "z", axis=0, tiled=True)
+    near = near.reshape(-1, *packed_shape)
     far = shifted(near, "core", 1)
     outs = [out_weight] + [shifted(out_weight, "tp", k) for k in range(1, members)]
 
-    keys_here = 2 * near.shape[0]
+    keys_here = 2 * near.shape[0] * own
     blocks = members * nope_width // LANES
     part = (blocks + 1, own, LANES)
 
@@ -328,6 +382,8 @@
             scratch_shapes=[
                 pltpu.VMEM((blocks + 1, rows, LANES), BF),
                 pltpu.VMEM((2 * rows, 2 * LANES), BF),
+                pltpu.VMEM((keys_here, rank), BF),
+                pltpu.VMEM((keys_here, LANES), BF),
                 pltpu.VMEM((keys_here, 2 * LANES), BF),
                 pltpu.VMEM((2 * rows, keys_here), F32),
                 pltpu.VMEM((2 * rows, LANES), F32),
@@ -389,21 +445,18 @@
     far_b = shifted(far_b, "tp", 1)
     from_above_b = shifted(down_b, "tp", -1)
     from_below_a = shifted(up_a, "tp", 1)
-    from_above_a = shifted((down_a.astype(F32) + far_a.astype(F32)).astype(BF), "tp", -1)
-    from_below_b = shifted((up_b.astype(F32) + far_b.astype(F32)).astype(BF), "tp", 1)
-
-    def added(base, *more):
-        for one in more:
-            base = base + one.astype(F32)
-        return base.astype(BF)
-
-    return jnp.concatenate(
-        [
-            added(mixed[:, :half], mine_a, from_above_a, from_below_a),
-            added(mixed[:, half:], mine_b, from_above_b, from_below_b),
-        ],
-        axis=1,
-    )
+    sum_b = (up_b.astype(F32) + far_b.astype(F32)).astype(BF)
+    from_below_b = shifted(sum_b, "tp", 1)
+    sum_a = (down_a.astype(F32) + far_a.astype(F32)).astype(BF)
+    from_above_a = shifted(sum_a, "tp", -1)
+    return pl.pallas_call(
+        close_body,
+        in_specs=[pl.BlockSpec(memory_space=pltpu.VMEM)] * 7,
+        out_specs=pl.BlockSpec(memory_space=pltpu.VMEM),
+        out_shape=jax.ShapeDtypeStruct((own, model), BF),
+        compiler_params=room(8),
+        name="close",
+    )(mixed, mine_a, from_above_a, from_below_a, mine_b, from_above_b, from_below_b)
 
 
 def solution(mesh):

time: 234 us -> 238 us (1.017)
  waiting for transfers between devices: 55.4 us -> 86.5 us
  starting transfers between devices: 49.9 us -> 32.7 us
  blocking collectives: 67.3 us -> 59.3 us
  local copies, waits for them, and re-layouts: 3.1 us -> 0.17 us
    ppermute x22, waiting for transfers between devices: 55.4 us -> 86.5 us  [shifted(): lax.ppermute(array, axis, [(i, (i + step) % count) for i in range(count)])]
    ppermute x22, starting transfers between devices: 49.9 us -> 32.7 us  [shifted(): lax.ppermute(array, axis, [(i, (i + step) % count) for i in range(count)])]
    all_gather x1, blocking collectives: 67.3 us -> 59.3 us  [layer(): near = lax.all_gather(packed, 'z', axis=0, tiled=True)]
    unnamed x21 -> x23, local copies, waits for them, and re-layouts: 3.1 us -> 0.17 us
  transfers between devices with their start and end apart: 23 -> 23, of which waited for: 11 -> 9; matrix products, arithmetic and copies ran while one was open for 0% -> 0% of each run, Pallas kernels for 13% -> 13%
where the time goes in v3:
time: 238 us; the launch traced here: 237 us
  waiting for transfers between devices  86.5 us (36%)
  blocking collectives  59.3 us (25%)
  Pallas kernels  42.8 us (18%)
  starting transfers between devices  32.7 us (14%)
  between operations  13.6 us (6%)
    ppermute x22, waiting for transfers between devices, shifted(): lax.ppermute(array, axis, [(i, (i + step) % count) for i in range(count)])  86.5 us
    all_gather x1, blocking collectives, layer(): near = lax.all_gather(packed, 'z', axis=0, tiled=True)  59.3 us
    ppermute x22, starting transfers between devices, shifted(): lax.ppermute(array, axis, [(i, (i + step) % count) for i in range(count)])  32.7 us
    pallas_call x1, Pallas kernels, layer(): pl.pallas_call(attend_body, grid_spec=pltpu.PrefetchScalarGridSpec(num_sc...  27.8 us
    pallas_call x1, Pallas kernels, layer(): pl.pallas_call(feed_body, in_specs=[pl.BlockSpec(memory_space=pltpu.VMEM)...  10.5 us
  transfers between devices with their start and end apart: 23, of which 9 were waited for; matrix products, arithmetic and copies ran while one was open for 0% of the time, Pallas kernels for 13%

profile of v3, /device:TPU:40, one launch (start us, length us, event | category | flops | bytes accessed | tf_op | source)
XLA Modules:
  0.0 237.5 jit_solution(5352614171376910448)
XLA Ops:
  6.6 2.1 pad_maximum_fusion
  8.8 0.1 copy.15.key
  9.0 0.1 pad_add_fusion.at
  9.1 1.3 prepare.1
  10.4 59.3 %all_gather.6 = bf16[3072,128]{1,0:T(8,128)(2,1)S(1)} all-gather(bf16[192,128]{1,0:T(8,128)(2,1)S(1)} %get-tuple-element.23), channel_id=1, replica_groups=mesh['grp'=2,'z'=16,'core'=2,'tp'=4] {'z'}, dimensions={0}, use_global_device_ids=true | all-gather | bytes 835584 | tf_op jit(solution)/shard_map/all_gather | solution.py:361
  69.7 2.0 collective-permute-start
  71.8 1.5 collective-permute-start.7
  73.2 1.8 collective-permute-start.8
  75.0 2.5 %collective-permute-start.9 = (bf16[256,2048]{1,0:T(8,128)(2,1)S(1)}, bf16[256,2048]{1,0:T(8,128)(2,1)S(1)}, u32[]{:S(2)}, u32[]{:S(2)}) collective-permute-start(bf16[256,2048]{1,0:T(8,128)(2,1)S(1)} %copy-done.1), channel_id=1, source_target_pairs={{0,3},{1,0},{2,1},{3,2},{4,7},{5,4},{6,5},{7,6},{8,11},{9,8},{10,9... | collective-permute-start | bytes 3145736 | tf_op jit(solution)/shard_map/ppermute | solution.py:28
  77.5 2.7 %collective-permute-done.q1 = bf16[320,384]{1,0:T(8,128)(2,1)S(1)} collective-permute-done((bf16[320,384]{1,0:T(8,128)(2,1)S(1)}, bf16[320,384]{1,0:T(8,128)(2,1)S(1)}, u32[]{:S(2)}, u32[]{:S(2)}) %collective-permute-start) | collective-permute-done | bytes 245792 | tf_op jit(solution)/shard_map/ppermute | solution.py:28
  80.2 1.9 collective-permute-start.1
  82.1 49.2 %collective-permute-done.1.q2 = bf16[320,384]{1,0:T(8,128)(2,1)S(1)} collective-permute-done((bf16[320,384]{1,0:T(8,128)(2,1)S(1)}, bf16[320,384]{1,0:T(8,128)(2,1)S(1)}, u32[]{:S(2)}, u32[]{:S(2)}) %collective-permute-start.1) | collective-permute-done | bytes 245792 | tf_op jit(solution)/shard_map/ppermute | solution.py:28
  131.3 7.4 %collective-permute-done.2.q3 = bf16[320,384]{1,0:T(8,128)(2,1)S(1)} collective-permute-done((bf16[320,384]{1,0:T(8,128)(2,1)S(1)}, bf16[320,384]{1,0:T(8,128)(2,1)S(1)}, u32[]{:S(2)}, u32[]{:S(2)}) %collective-permute-start.2) | collective-permute-done | bytes 245792 | tf_op jit(solution)/shard_map/ppermute | solution.py:28
  138.7 27.8 %attend.1 = (bf16[9,80,128]{2,1,0:T(8,128)(2,1)S(1)}, bf16[9,80,128]{2,1,0:T(8,128)(2,1)S(1)}, bf16[9,80,128]{2,1,0:T(8,128)(2,1)S(1)}, bf16[9,80,128]{2,1,0:T(8,128)(2,1)S(1)}) custom-call(s32[2]{0:T(128)S(1)} %pad_add_fusion.at, bf16[320,384]{1,0:T(8,128)(2,1)S(1)} %get-tuple-element.22.q0, bf16[320,384]{1,0:T(8,128)(2,1)S(1)} %collective-permute-done.q1, ...), custom_call_target="tpu_custom_call" | custom-call | tf_op jit(solution)/shard_map/attend/pallas_call | solution.py:373
  166.5 0.1 collective-permute-start.4
  166.6 3.0 %collective-permute-start.5 = (bf16[9,80,128]{2,1,0:T(8,128)(2,1)S(1)}, bf16[9,80,128]{2,1,0:T(8,128)(2,1)S(1)}, u32[]{:S(2)}, u32[]{:S(2)}) collective-permute-start(bf16[9,80,128]{2,1,0:T(8,128)(2,1)S(1)} %get-tuple-element.26), channel_id=1, source_target_pairs={{0,2},{1,3},{2,0},{3,1},{4,6},{5,7},{6,4},{7,5},{8,10},{9,11},{10,... | collective-permute-start | bytes 552968 | tf_op jit(solution)/shard_map/ppermute | solution.py:28
  169.6 7.6 %collective-permute-done.4.p1 = bf16[9,80,128]{2,1,0:T(8,128)(2,1)S(1)} collective-permute-done((bf16[9,80,128]{2,1,0:T(8,128)(2,1)S(1)}, bf16[9,80,128]{2,1,0:T(8,128)(2,1)S(1)}, u32[]{:S(2)}, u32[]{:S(2)}) %collective-permute-start.4) | collective-permute-done | bytes 184352 | tf_op jit(solution)/shard_map/ppermute | solution.py:28
  177.2 6.7 %collective-permute-done.6.p3 = bf16[9,80,128]{2,1,0:T(8,128)(2,1)S(1)} collective-permute-done((bf16[9,80,128]{2,1,0:T(8,128)(2,1)S(1)}, bf16[9,80,128]{2,1,0:T(8,128)(2,1)S(1)}, u32[]{:S(2)}, u32[]{:S(2)}) %collective-permute-start.6) | collective-permute-done | bytes 184352 | tf_op jit(solution)/shard_map/ppermute | solution.py:28
  183.9 2.3 merge.1
  186.2 0.1 collective-permute-start.10
  186.4 3.2 %collective-permute-start.13 = (bf16[80,1024]{1,0:T(8,128)(2,1)S(1)}, bf16[80,1024]{1,0:T(8,128)(2,1)S(1)}, u32[]{:S(2)}, u32[]{:S(2)}) collective-permute-start(bf16[80,1024]{1,0:T(8,128)(2,1)S(1)} %get-tuple-element.30.refs_1_), channel_id=1, source_target_pairs={{0,3},{1,0},{2,1},{3,2},{4,7},{5,4},{6,5},{7,6},{8,11},{9,8},{10,9... | collective-permute-start | bytes 491528 | tf_op jit(solution)/shard_map/ppermute | solution.py:28
  189.6 3.2 %collective-permute-start.15 = (bf16[80,1024]{1,0:T(8,128)(2,1)S(1)}, bf16[80,1024]{1,0:T(8,128)(2,1)S(1)}, u32[]{:S(2)}, u32[]{:S(2)}) collective-permute-start(bf16[80,1024]{1,0:T(8,128)(2,1)S(1)} %get-tuple-element.29.refs_0_), channel_id=1, source_target_pairs={{0,3},{1,0},{2,1},{3,2},{4,7},{5,4},{6,5},{7,6},{8,11},{9,8},{10,9... | collective-permute-start | bytes 491528 | tf_op jit(solution)/shard_map/ppermute | solution.py:28
  192.9 3.2 %collective-permute-start.14 = (bf16[80,1024]{1,0:T(8,128)(2,1)S(1)}, bf16[80,1024]{1,0:T(8,128)(2,1)S(1)}, u32[]{:S(2)}, u32[]{:S(2)}) collective-permute-start(bf16[80,1024]{1,0:T(8,128)(2,1)S(1)} %collective-permute-done.13.refs_7_), channel_id=1, source_target_pairs={{0,3},{1,0},{2,1},{3,2},{4,7},{5,4},{6,5},{7,6},{8,11},{9,8},{10,9... | collective-permute-start | bytes 491528 | tf_op jit(solution)/shard_map/ppermute | solution.py:28
  196.1 3.3 %collective-permute-done.12.refs_4_ = bf16[80,1024]{1,0:T(8,128)(2,1)S(1)} collective-permute-done((bf16[80,1024]{1,0:T(8,128)(2,1)S(1)}, bf16[80,1024]{1,0:T(8,128)(2,1)S(1)}, u32[]{:S(2)}, u32[]{:S(2)}) %collective-permute-start.12) | collective-permute-done | bytes 163872 | tf_op jit(solution)/shard_map/ppermute | solution.py:28
  199.4 10.5 %feed.1 = (bf16[80,1024]{1,0:T(8,128)(2,1)S(1)}, bf16[80,1024]{1,0:T(8,128)(2,1)S(1)}, bf16[80,1024]{1,0:T(8,128)(2,1)S(1)}, bf16[80,1024]{1,0:T(8,128)(2,1)S(1)...) custom-call(bf16[80,1024]{1,0:T(8,128)(2,1)S(1)} %get-tuple-element., ...), custom_call_target="tpu_custom_call" | custom-call | tf_op jit(solution)/shard_map/feed/pallas_call | solution.py:427
  209.9 3.3 %collective-permute-start.16 = (bf16[80,1024]{1,0:T(8,128)(2,1)S(1)}, bf16[80,1024]{1,0:T(8,128)(2,1)S(1)}, u32[]{:S(2)}, u32[]{:S(2)}) collective-permute-start(bf16[80,1024]{1,0:T(8,128)(2,1)S(1)} %get-tuple-element.33), channel_id=1, source_target_pairs={{0,3},{1,0},{2,1},{3,2},{4,7},{5,4},{6,5},{7,6},{8,11},{9,8},{10,9... | collective-permute-start | bytes 491528 | tf_op jit(solution)/shard_map/ppermute | solution.py:28
  213.3 3.2 %collective-permute-start.19 = (bf16[80,1024]{1,0:T(8,128)(2,1)S(1)}, bf16[80,1024]{1,0:T(8,128)(2,1)S(1)}, u32[]{:S(2)}, u32[]{:S(2)}) collective-permute-start(bf16[80,1024]{1,0:T(8,128)(2,1)S(1)} %get-tuple-element.36), channel_id=1, source_target_pairs={{0,3},{1,0},{2,1},{3,2},{4,7},{5,4},{6,5},{7,6},{8,11},{9,8},{10,9... | collective-permute-start | bytes 491528 | tf_op jit(solution)/shard_map/ppermute | solution.py:28
  216.6 3.4 %collective-permute-start.17 = (bf16[80,1024]{1,0:T(8,128)(2,1)S(1)}, bf16[80,1024]{1,0:T(8,128)(2,1)S(1)}, u32[]{:S(2)}, u32[]{:S(2)}) collective-permute-start(bf16[80,1024]{1,0:T(8,128)(2,1)S(1)} %add_convert_fusion.1), channel_id=1, source_target_pairs={{0,3},{1,0},{2,1},{3,2},{4,7},{5,4},{6,5},{7,6},{8,11},{9,8},{10,9... | collective-permute-start | bytes 491528 | tf_op jit(solution)/shard_map/ppermute | solution.py:28
  220.0 3.1 %collective-permute-done.20 = bf16[80,1024]{1,0:T(8,128)(2,1)S(1)} collective-permute-done((bf16[80,1024]{1,0:T(8,128)(2,1)S(1)}, bf16[80,1024]{1,0:T(8,128)(2,1)S(1)}, u32[]{:S(2)}, u32[]{:S(2)}) %collective-permute-start.20) | collective-permute-done | bytes 163872 | tf_op jit(solution)/shard_map/ppermute | solution.py:28
  223.1 0.1 collective-permute-start.21
  223.3 6.5 %collective-permute-done.21.b2 = bf16[80,1024]{1,0:T(8,128)(2,1)S(1)} collective-permute-done((bf16[80,1024]{1,0:T(8,128)(2,1)S(1)}, bf16[80,1024]{1,0:T(8,128)(2,1)S(1)}, u32[]{:S(2)}, u32[]{:S(2)}) %collective-permute-start.21) | collective-permute-done | bytes 163872 | tf_op jit(solution)/shard_map/ppermute | solution.py:28
  229.8 0.9 close.1
  (48 shorter events, 0.3 us)
Async XLA Ops:
  6.5 2.5 %copy-start.9 = (f32[1,128]{1,0:T(1,128)S(1)}, f32[1,128]{1,0:T(1,128)}, u32[]{:S(2)}) copy-start(f32[1,128]{1,0:T(1,128)} %constant.18.clone.inverse) | copy-start | bytes 1540
  6.6 2.5 %copy-start.8 = (f32[256]{0:T(256)S(1)}, f32[256]{0:T(256)}, u32[]{:S(2)}) copy-start(f32[256]{0:T(256)} %param.18) | copy-start | bytes 3076
  6.6 2.5 %copy-start.5 = (bf16[320,256]{1,0:T(8,128)(2,1)S(1)}, bf16[320,256]{1,0:T(8,128)(2,1)}, u32[]{:S(2)}) copy-start(bf16[320,256]{1,0:T(8,128)(2,1)} %nope.1) | copy-start | bytes 491524
  6.6 2.5 %copy-start.6 = (bf16[320,128]{1,0:T(8,128)(2,1)S(1)}, bf16[320,128]{1,0:T(8,128)(2,1)}, u32[]{:S(2)}) copy-start(bf16[320,128]{1,0:T(8,128)(2,1)} %rope.1) | copy-start | bytes 245764
  6.6 192.9 %all-gather.2.cloned.1.call-start = ((), (), s32[]{:S(2)}) async-start(), calls=%async_computation | async-start | bytes 17842176 | tf_op jit(solution)/shard_map/all_gather | solution.py:330
  6.6 132.0 %copy-start.3 = (bf16[256,1024]{1,0:T(8,128)(2,1)S(1)}, bf16[256,1024]{1,0:T(8,128)(2,1)}, u32[]{:S(2)}) copy-start(bf16[256,1024]{1,0:T(8,128)(2,1)} %value_w.1) | copy-start | bytes 1572868
  8.8 63.0 %copy-start.1 = (bf16[256,2048]{1,0:T(8,128)(2,1)S(1)}, bf16[256,2048]{1,0:T(8,128)(2,1)}, u32[]{:S(2)}) copy-start(bf16[256,2048]{1,0:T(8,128)(2,1)} %w0.1) | copy-start | bytes 3145732
  8.8 129.9 %copy-start.2 = (bf16[256,1024]{1,0:T(8,128)(2,1)S(1)}, bf16[256,1024]{1,0:T(8,128)(2,1)}, u32[]{:S(2)}) copy-start(bf16[256,1024]{1,0:T(8,128)(2,1)} %key_w.1) | copy-start | bytes 1572868
  69.7 69.0 %collective-permute-start.3 = (bf16[16,192,128]{2,1,0:T(8,128)(2,1)S(1)}, bf16[16,192,128]{2,1,0:T(8,128)(2,1)S(1)}, u32[]{:S(2)}, u32[]{:S(2)}) collective-permute-start(bf16[16,192,128]{2,1,0:T(8,128)(2,1)S(1)} %bitcast.7), channel_id=1, source_target_pairs={{0,4},{4,0},{1,5},{5,1},{2,6},{6,2},{3,7},{7,3},{8,12},{12,8},{9,1... | collective-permute-start | bytes 2359304 | tf_op jit(solution)/shard_map/ppermute | solution.py:28
  69.7 114.2 %copy-start = (bf16[320,2048]{1,0:T(8,128)(2,1)S(1)}, bf16[320,2048]{1,0:T(8,128)(2,1)}, u32[]{:S(2)}) copy-start(bf16[320,2048]{1,0:T(8,128)(2,1)} %residual.1) | copy-start | bytes 3932164
  69.7 114.2 %copy-start.7 = (f32[2048]{0:T(1024)S(1)}, f32[2048]{0:T(1024)}, u32[]{:S(2)}) copy-start(f32[2048]{0:T(1024)} %param.23) | copy-start | bytes 24580
  69.7 10.5 %collective-permute-start = (bf16[320,384]{1,0:T(8,128)(2,1)S(1)}, bf16[320,384]{1,0:T(8,128)(2,1)S(1)}, u32[]{:S(2)}, u32[]{:S(2)}) collective-permute-start(bf16[320,384]{1,0:T(8,128)(2,1)S(1)} %get-tuple-element.22.q0), channel_id=1, source_target_pairs={{0,1},{1,2},{2,3},{3,0},{4,5},{5,6},{6,7},{7,4},{8,9},{9,10},{10,1... | collective-permute-start | bytes 737288 | tf_op jit(solution)/shard_map/ppermute | solution.py:28
  71.8 112.1 %collective-permute-start.7 = (bf16[256,2048]{1,0:T(8,128)(2,1)S(1)}, bf16[256,2048]{1,0:T(8,128)(2,1)S(1)}, u32[]{:S(2)}, u32[]{:S(2)}) collective-permute-start(bf16[256,2048]{1,0:T(8,128)(2,1)S(1)} %copy-done.1), channel_id=1, source_target_pairs={{0,1},{1,2},{2,3},{3,0},{4,5},{5,6},{6,7},{7,4},{8,9},{9,10},{10,1... | collective-permute-start | bytes 3145736 | tf_op jit(solution)/shard_map/ppermute | solution.py:28
  73.2 110.6 %collective-permute-start.8 = (bf16[256,2048]{1,0:T(8,128)(2,1)S(1)}, bf16[256,2048]{1,0:T(8,128)(2,1)S(1)}, u32[]{:S(2)}, u32[]{:S(2)}) collective-permute-start(bf16[256,2048]{1,0:T(8,128)(2,1)S(1)} %copy-done.1), channel_id=1, source_target_pairs={{0,2},{1,3},{2,0},{3,1},{4,6},{5,7},{6,4},{7,5},{8,10},{9,11},{10,... | collective-permute-start | bytes 3145736 | tf_op jit(solution)/shard_map/ppermute | solution.py:28
  75.0 108.9 %collective-permute-start.9 = (bf16[256,2048]{1,0:T(8,128)(2,1)S(1)}, bf16[256,2048]{1,0:T(8,128)(2,1)S(1)}, u32[]{:S(2)}, u32[]{:S(2)}) collective-permute-start(bf16[256,2048]{1,0:T(8,128)(2,1)S(1)} %copy-done.1), channel_id=1, source_target_pairs={{0,3},{1,0},{2,1},{3,2},{4,7},{5,4},{6,5},{7,6},{8,11},{9,8},{10,9... | collective-permute-start | bytes 3145736 | tf_op jit(solution)/shard_map/ppermute | solution.py:28
  80.2 51.1 %collective-permute-start.1 = (bf16[320,384]{1,0:T(8,128)(2,1)S(1)}, bf16[320,384]{1,0:T(8,128)(2,1)S(1)}, u32[]{:S(2)}, u32[]{:S(2)}) collective-permute-start(bf16[320,384]{1,0:T(8,128)(2,1)S(1)} %get-tuple-element.22.q0), channel_id=1, source_target_pairs={{0,2},{1,3},{2,0},{3,1},{4,6},{5,7},{6,4},{7,5},{8,10},{9,11},{10,... | collective-permute-start | bytes 737288 | tf_op jit(solution)/shard_map/ppermute | solution.py:28
  131.3 7.4 %collective-permute-start.2 = (bf16[320,384]{1,0:T(8,128)(2,1)S(1)}, bf16[320,384]{1,0:T(8,128)(2,1)S(1)}, u32[]{:S(2)}, u32[]{:S(2)}) collective-permute-start(bf16[320,384]{1,0:T(8,128)(2,1)S(1)} %get-tuple-element.22.q0), channel_id=1, source_target_pairs={{0,3},{1,0},{2,1},{3,2},{4,7},{5,4},{6,5},{7,6},{8,11},{9,8},{10,9... | collective-permute-start | bytes 737288 | tf_op jit(solution)/shard_map/ppermute | solution.py:28
  166.5 10.7 %collective-permute-start.4 = (bf16[9,80,128]{2,1,0:T(8,128)(2,1)S(1)}, bf16[9,80,128]{2,1,0:T(8,128)(2,1)S(1)}, u32[]{:S(2)}, u32[]{:S(2)}) collective-permute-start(bf16[9,80,128]{2,1,0:T(8,128)(2,1)S(1)} %get-tuple-element.25), channel_id=1, source_target_pairs={{0,1},{1,2},{2,3},{3,0},{4,5},{5,6},{6,7},{7,4},{8,9},{9,10},{10,1... | collective-permute-start | bytes 552968 | tf_op jit(solution)/shard_map/ppermute | solution.py:28
  166.6 10.5 %collective-permute-start.5 = (bf16[9,80,128]{2,1,0:T(8,128)(2,1)S(1)}, bf16[9,80,128]{2,1,0:T(8,128)(2,1)S(1)}, u32[]{:S(2)}, u32[]{:S(2)}) collective-permute-start(bf16[9,80,128]{2,1,0:T(8,128)(2,1)S(1)} %get-tuple-element.26), channel_id=1, source_target_pairs={{0,2},{1,3},{2,0},{3,1},{4,6},{5,7},{6,4},{7,5},{8,10},{9,11},{10,... | collective-permute-start | bytes 552968 | tf_op jit(solution)/shard_map/ppermute | solution.py:28
  177.2 6.7 %collective-permute-start.6 = (bf16[9,80,128]{2,1,0:T(8,128)(2,1)S(1)}, bf16[9,80,128]{2,1,0:T(8,128)(2,1)S(1)}, u32[]{:S(2)}, u32[]{:S(2)}) collective-permute-start(bf16[9,80,128]{2,1,0:T(8,128)(2,1)S(1)} %get-tuple-element.27), channel_id=1, source_target_pairs={{0,3},{1,0},{2,1},{3,2},{4,7},{5,4},{6,5},{7,6},{8,11},{9,8},{10,9... | collective-permute-start | bytes 552968 | tf_op jit(solution)/shard_map/ppermute | solution.py:28
  186.2 6.6 %collective-permute-start.10 = (bf16[80,1024]{1,0:T(8,128)(2,1)S(1)}, bf16[80,1024]{1,0:T(8,128)(2,1)S(1)}, u32[]{:S(2)}, u32[]{:S(2)}) collective-permute-start(bf16[80,1024]{1,0:T(8,128)(2,1)S(1)} %get-tuple-element.29.refs_0_), channel_id=1, source_target_pairs={{0,1},{1,2},{2,3},{3,0},{4,5},{5,6},{6,7},{7,4},{8,9},{9,10},{10,1... | collective-permute-start | bytes 491528 | tf_op jit(solution)/shard_map/ppermute | solution.py:28
  186.4 6.5 %collective-permute-start.13 = (bf16[80,1024]{1,0:T(8,128)(2,1)S(1)}, bf16[80,1024]{1,0:T(8,128)(2,1)S(1)}, u32[]{:S(2)}, u32[]{:S(2)}) collective-permute-start(bf16[80,1024]{1,0:T(8,128)(2,1)S(1)} %get-tuple-element.30.refs_1_), channel_id=1, source_target_pairs={{0,3},{1,0},{2,1},{3,2},{4,7},{5,4},{6,5},{7,6},{8,11},{9,8},{10,9... | collective-permute-start | bytes 491528 | tf_op jit(solution)/shard_map/ppermute | solution.py:28
  189.6 6.5 %collective-permute-start.11 = (bf16[80,1024]{1,0:T(8,128)(2,1)S(1)}, bf16[80,1024]{1,0:T(8,128)(2,1)S(1)}, u32[]{:S(2)}, u32[]{:S(2)}) collective-permute-start(bf16[80,1024]{1,0:T(8,128)(2,1)S(1)} %get-tuple-element.30.refs_1_), channel_id=1, source_target_pairs={{0,1},{1,2},{2,3},{3,0},{4,5},{5,6},{6,7},{7,4},{8,9},{9,10},{10,1... | collective-permute-start | bytes 491528 | tf_op jit(solution)/shard_map/ppermute | solution.py:28
  189.6 6.5 %collective-permute-start.15 = (bf16[80,1024]{1,0:T(8,128)(2,1)S(1)}, bf16[80,1024]{1,0:T(8,128)(2,1)S(1)}, u32[]{:S(2)}, u32[]{:S(2)}) collective-permute-start(bf16[80,1024]{1,0:T(8,128)(2,1)S(1)} %get-tuple-element.29.refs_0_), channel_id=1, source_target_pairs={{0,3},{1,0},{2,1},{3,2},{4,7},{5,4},{6,5},{7,6},{8,11},{9,8},{10,9... | collective-permute-start | bytes 491528 | tf_op jit(solution)/shard_map/ppermute | solution.py:28
  192.9 6.5 %collective-permute-start.12 = (bf16[80,1024]{1,0:T(8,128)(2,1)S(1)}, bf16[80,1024]{1,0:T(8,128)(2,1)S(1)}, u32[]{:S(2)}, u32[]{:S(2)}) collective-permute-start(bf16[80,1024]{1,0:T(8,128)(2,1)S(1)} %collective-permute-done.10.refs_2_), channel_id=1, source_target_pairs={{0,1},{1,2},{2,3},{3,0},{4,5},{5,6},{6,7},{7,4},{8,9},{9,10},{10,1... | collective-permute-start | bytes 491528 | tf_op jit(solution)/shard_map/ppermute | solution.py:28
  192.9 6.5 %collective-permute-start.14 = (bf16[80,1024]{1,0:T(8,128)(2,1)S(1)}, bf16[80,1024]{1,0:T(8,128)(2,1)S(1)}, u32[]{:S(2)}, u32[]{:S(2)}) collective-permute-start(bf16[80,1024]{1,0:T(8,128)(2,1)S(1)} %collective-permute-done.13.refs_7_), channel_id=1, source_target_pairs={{0,3},{1,0},{2,1},{3,2},{4,7},{5,4},{6,5},{7,6},{8,11},{9,8},{10,9... | collective-permute-start | bytes 491528 | tf_op jit(solution)/shard_map/ppermute | solution.py:28
  209.9 6.6 %collective-permute-start.16 = (bf16[80,1024]{1,0:T(8,128)(2,1)S(1)}, bf16[80,1024]{1,0:T(8,128)(2,1)S(1)}, u32[]{:S(2)}, u32[]{:S(2)}) collective-permute-start(bf16[80,1024]{1,0:T(8,128)(2,1)S(1)} %get-tuple-element.33), channel_id=1, source_target_pairs={{0,3},{1,0},{2,1},{3,2},{4,7},{5,4},{6,5},{7,6},{8,11},{9,8},{10,9... | collective-permute-start | bytes 491528 | tf_op jit(solution)/shard_map/ppermute | solution.py:28
  213.3 10.0 %collective-permute-start.18 = (bf16[80,1024]{1,0:T(8,128)(2,1)S(1)}, bf16[80,1024]{1,0:T(8,128)(2,1)S(1)}, u32[]{:S(2)}, u32[]{:S(2)}) collective-permute-start(bf16[80,1024]{1,0:T(8,128)(2,1)S(1)} %get-tuple-element.34), channel_id=1, source_target_pairs={{0,1},{1,2},{2,3},{3,0},{4,5},{5,6},{6,7},{7,4},{8,9},{9,10},{10,1... | collective-permute-start | bytes 491528 | tf_op jit(solution)/shard_map/ppermute | solution.py:28
  213.3 10.0 %collective-permute-start.19 = (bf16[80,1024]{1,0:T(8,128)(2,1)S(1)}, bf16[80,1024]{1,0:T(8,128)(2,1)S(1)}, u32[]{:S(2)}, u32[]{:S(2)}) collective-permute-start(bf16[80,1024]{1,0:T(8,128)(2,1)S(1)} %get-tuple-element.36), channel_id=1, source_target_pairs={{0,3},{1,0},{2,1},{3,2},{4,7},{5,4},{6,5},{7,6},{8,11},{9,8},{10,9... | collective-permute-start | bytes 491528 | tf_op jit(solution)/shard_map/ppermute | solution.py:28
  216.5 6.5 %collective-permute-start.20 = (bf16[80,1024]{1,0:T(8,128)(2,1)S(1)}, bf16[80,1024]{1,0:T(8,128)(2,1)S(1)}, u32[]{:S(2)}, u32[]{:S(2)}) collective-permute-start(bf16[80,1024]{1,0:T(8,128)(2,1)S(1)} %get-tuple-element.38), channel_id=1, source_target_pairs={{0,1},{1,2},{2,3},{3,0},{4,5},{5,6},{6,7},{7,4},{8,9},{9,10},{10,1... | collective-permute-start | bytes 491528 | tf_op jit(solution)/shard_map/ppermute | solution.py:28
  216.6 6.7 %collective-permute-start.17 = (bf16[80,1024]{1,0:T(8,128)(2,1)S(1)}, bf16[80,1024]{1,0:T(8,128)(2,1)S(1)}, u32[]{:S(2)}, u32[]{:S(2)}) collective-permute-start(bf16[80,1024]{1,0:T(8,128)(2,1)S(1)} %add_convert_fusion.1), channel_id=1, source_target_pairs={{0,3},{1,0},{2,1},{3,2},{4,7},{5,4},{6,5},{7,6},{8,11},{9,8},{10,9... | collective-permute-start | bytes 491528 | tf_op jit(solution)/shard_map/ppermute | solution.py:28
  223.1 6.6 %collective-permute-start.21 = (bf16[80,1024]{1,0:T(8,128)(2,1)S(1)}, bf16[80,1024]{1,0:T(8,128)(2,1)S(1)}, u32[]{:S(2)}, u32[]{:S(2)}) collective-permute-start(bf16[80,1024]{1,0:T(8,128)(2,1)S(1)} %add_convert_fusion), channel_id=1, source_target_pairs={{0,1},{1,2},{2,3},{3,0},{4,5},{5,6},{6,7},{7,4},{8,9},{9,10},{10,1... | collective-permute-start | bytes 491528 | tf_op jit(solution)/shard_map/ppermute | solution.py:28
  (2 other events, 4.8 us)
Sparse Core Ops, SparseCore 0:
  9.3 126.4 all-gather.1
